TPU v7x, 512 devices: a whole 4x8x8 slice. The times are simulated.
512 devices in a mesh: sp: 64 (over z, y), tp: 8 (over x, core).
Axes of the slice: x: 4, y: 8, z: 8, core: 2. Of those that a mesh axis runs over, the one named last changes fastest.
Arguments:
- tokens: bfloat16 [65536, 2048], P('sp'), may hold values from -6 to 6
- norm_gain: float32 [2048], replicated, may hold values from 0.1 to 1.9
- w_query: bfloat16 [2048, 512], P(None, 'tp'), may hold values from -0.79549513 to 0.79549513
- w_key: bfloat16 [2048, 128], P('sp'), may hold values from -0.79549513 to 0.79549513
- w_value: bfloat16 [2048, 128], P('sp'), may hold values from -0.125 to 0.125
- w_pool_in: bfloat16 [2048, 512], P(None, 'tp'), may hold values from -0.125 to 0.125
- sink_logit: float32 [8], P('tp'), may hold values from 3 to 7
- pool_scale: float32 [512], P('tp'), may hold values from 0.05 to 0.5
- w_out: bfloat16 [1024, 2048], P('tp', 'sp'), may hold values from -0.75 to 0.75
Outputs:
- mixed_out: bfloat16 [65536, 2048], P(('sp', 'tp'))
All inputs are finite; a program needn't handle non-finite values.
Results may differ from a plain program's by a relative error of at most 0.03.
The roundings to bfloat16 on the way count: a program that leaves them out, or rounds other values in their place, can miss the bound.
Values may be sent and summed in bfloat16 or wider, within the bound.
A program may use at most 64 MiB of HBM per device.

v0:
```python
import jax
import jax.numpy as jnp
from jax import lax
from jax.sharding import PartitionSpec as P

HEAD = 64
QH = 8
KVH = 2
POOL_CH = 128
WINDOW = 128
QB = 128


NEG_BIG = -1e30
POOL_SPANS = (2, 4, 8, 16)


def in_one_piece(arrays, axis, dim, along):
    both = jnp.concatenate(arrays, axis=along)
    filled, at, finished = (lax.all_gather(both, axis, axis=dim, tiled=True), 0, [])
    for a in arrays:
        finished.append(lax.slice_in_dim(filled, at, at + a.shape[along], axis=along))
        at += a.shape[along]
    return tuple(finished)


def extended(block, sides, width):
    for axis, dim in sides:
        count = lax.axis_size(axis)
        forward = [(i, i + 1) for i in range(count - 1)]
        backward = [(target, source) for source, target in forward]
        low = lax.ppermute(
            lax.slice_in_dim(block, block.shape[dim] - width, None, axis=dim), axis, forward
        )
        high = lax.ppermute(lax.slice_in_dim(block, 0, width, axis=dim), axis, backward)
        block = jnp.concatenate([low, block, high], axis=dim)
    return block


def rows_first(arrays, axis, dims):
    turned = [jnp.moveaxis(a, dim, 0) for a, dim in zip(arrays, dims)]
    both = jnp.concatenate([t.reshape(len(t), -1) for t in turned], axis=1)
    filled, at, finished = (lax.all_gather(both, axis, axis=0, tiled=True), 0, [])
    for t, dim in zip(turned, dims):
        section = filled[:, at : at + t[0].size].reshape(-1, *t.shape[1:])
        finished.append(jnp.moveaxis(section, 0, dim))
        at += t[0].size
    return tuple(finished)


def in_order(tiles, dim):
    tiles = jnp.moveaxis(tiles, 0, dim)
    shape = tiles.shape
    return tiles.reshape(*shape[:dim], shape[dim] * shape[dim + 1], *shape[dim + 2 :])


def from_everyone(x, axis):
    peers = lax.axis_size(axis)
    return lax.all_to_all(jnp.broadcast_to(x[None], (peers, *x.shape)), axis, 0, 0, tiled=True)


def collect(x, axis, dim):
    return in_order(from_everyone(x, axis), dim)


def layer_normed(tokens, norm_gain):
    values = tokens.astype(jnp.float32)
    center = jnp.mean(values, axis=-1, keepdims=True)
    spread = jnp.mean(jnp.square(values - center), axis=-1, keepdims=True)
    return ((values - center) * lax.rsqrt(spread + 1e-06) * norm_gain).astype(jnp.bfloat16)


def rotate(values, positions):
    half = HEAD // 2
    inverse = 10000.0 ** (-jnp.arange(half, dtype=jnp.float32) / half)
    angles = positions[:, None] * inverse[None, :]
    cosine = jnp.cos(angles)[:, None, :]
    sine = jnp.sin(angles)[:, None, :]
    first = values[..., :half]
    second = values[..., half:]
    return jnp.concatenate(
        [first * cosine - second * sine, first * sine + second * cosine], axis=-1
    )


def body(tokens, norm_gain, w_query, w_key, w_value, w_pool_in, sink_logit, pool_scale, w_out):
    local_rows = tokens.shape[0]
    seq_total = local_rows * lax.axis_size("sp")
    offset = lax.axis_index("sp") * local_rows
    tp_place = lax.axis_index("tp")
    local_heads = w_query.shape[1] // HEAD
    local_pool = w_pool_in.shape[1]
    reach = POOL_SPANS[-1] // 2
    normed = layer_normed(tokens, norm_gain)
    positions = (offset + jnp.arange(local_rows)).astype(jnp.float32)
    query = rotate(
        jnp.dot(normed, w_query, preferred_element_type=jnp.float32).reshape(
            local_rows, local_heads, HEAD
        ),
        positions,
    ).astype(jnp.bfloat16)
    key_head = tp_place * local_heads // (QH // KVH)
    key_cols = lax.dynamic_slice_in_dim(w_key, key_head * HEAD, HEAD, 1)
    value_cols = lax.dynamic_slice_in_dim(w_value, key_head * HEAD, HEAD, 1)
    pieces = in_one_piece((key_cols, value_cols), "sp", 0, 1)
    key_sum = jnp.dot(normed, pieces[0], preferred_element_type=jnp.float32)
    value_sum = jnp.dot(normed, pieces[1], preferred_element_type=jnp.float32)
    key = rotate(key_sum[:, None, :], positions)[:, 0, :].astype(jnp.bfloat16)
    value = value_sum.astype(jnp.bfloat16)
    key_value = jnp.concatenate([key, value], axis=1)
    pool_in = jnp.dot(normed, w_pool_in, preferred_element_type=jnp.float32).astype(jnp.bfloat16)
    widened = extended(jnp.concatenate([key_value, pool_in], axis=1), (("sp", 0),), WINDOW)
    kv_wide = widened[:, : 2 * HEAD]
    pool_wide = widened[WINDOW - reach : WINDOW + local_rows + reach, 2 * HEAD :]
    span = QB + 2 * WINDOW
    sink_here = sink_logit[:, None, None]
    results = []
    for block in range(local_rows // QB):
        queries = query[block * QB : (block + 1) * QB]
        keys = kv_wide[block * QB : block * QB + span, :HEAD]
        values = kv_wide[block * QB : block * QB + span, HEAD:]
        scores = jnp.einsum(
            "ihd,jd->hij", queries, keys, preferred_element_type=jnp.float32
        ) * HEAD ** (-0.5)
        query_pos = offset + block * QB + jnp.arange(QB)
        key_pos = offset + block * QB - WINDOW + jnp.arange(span)
        valid = (
            (jnp.abs(query_pos[:, None] - key_pos[None, :]) <= WINDOW)
            & (key_pos[None, :] >= 0)
            & (key_pos[None, :] < seq_total)
        )
        scores = jnp.where(valid, scores, NEG_BIG)
        highest = jnp.maximum(jnp.max(scores, axis=-1, keepdims=True), sink_here)
        expo = jnp.where(valid, jnp.exp(scores - highest), 0.0)
        total = jnp.sum(expo, axis=-1, keepdims=True) + jnp.exp(sink_here - highest)
        weights = (expo / total).astype(jnp.bfloat16)
        result = jnp.einsum("hij,jd->ihd", weights, values, preferred_element_type=jnp.float32)
        results.append(result.reshape(QB, local_heads * HEAD).astype(jnp.bfloat16))
    attended = jnp.concatenate(results, axis=0)
    pool_vals = pool_wide.astype(jnp.float32)
    window_sum = pool_vals
    global_pos = offset + jnp.arange(local_rows)
    channel = tp_place * local_pool + jnp.arange(local_pool)
    window_group = channel // POOL_CH
    measured = jnp.zeros((local_rows, local_pool), jnp.float32)
    stride = 1
    for index, width in enumerate(POOL_SPANS):
        window_sum = window_sum[:-stride] + window_sum[stride:]
        stride = width
        sums = window_sum[reach - width // 2 : reach - width // 2 + local_rows]
        counted = (
            jnp.minimum(global_pos + width // 2, seq_total)
            - jnp.maximum(global_pos - width // 2, 0)
        ).astype(jnp.float32)
        measured = measured + jnp.where(
            window_group[None, :] == index, sums / counted[:, None], 0.0
        )
    pooled = ((measured - pool_vals[reach : reach + local_rows]) * pool_scale).astype(jnp.bfloat16)
    attended_all, pooled_all = rows_first((attended, pooled), "tp", (1, 1))
    joined_all = jnp.concatenate([attended_all, pooled_all], axis=1)
    own_rows = collect(w_out, "sp", 1)
    column_block = lax.all_to_all(own_rows, "tp", split_axis=1, concat_axis=0, tiled=True)
    partial_cols = jnp.dot(joined_all, column_block, preferred_element_type=jnp.float32).astype(
        jnp.bfloat16
    )
    return lax.all_to_all(partial_cols, "tp", split_axis=0, concat_axis=1, tiled=True)


def solution(mesh):
    in_specs = (
        P("sp", None),
        P(),
        P(None, "tp"),
        P("sp", None),
        P("sp", None),
        P(None, "tp"),
        P("tp"),
        P("tp"),
        P("tp", "sp"),
    )
    out_specs = P(("sp", "tp"), None)
    return jax.shard_map(body, mesh=mesh, in_specs=in_specs, out_specs=out_specs, check_vma=False)
```

profile of v0, /device:TPU:1, one launch (start us, length us, event | category | flops | bytes accessed | tf_op | source)
XLA Modules:
  0.0 157.3 jit_solution(11905383082164041092)
XLA Ops:
  6.6 0.9 constant_dynamic-slice_fusion
  7.6 46.0 %all_gather.6 = bf16[2048,128]{1,0:T(8,128)(2,1)S(1)} all-gather(bf16[32,128]{1,0:T(8,128)(2,1)S(1)} %pad_maximum_fusion.22), channel_id=1, replica_groups=mesh['sp'=64,'tp'=8] {'sp'}, dimensions={0}, use_global_device_ids=true | all-gather | bytes 532480 | tf_op jit(solution)/shard_map/all_gather | solution.py:20
  53.6 2.8 %convert_reduce_fusion = f32[1024]{0:T(1024)S(1)} fusion(bf16[1024,2048]{1,0:T(8,128)(2,1)} %param.9), kind=kLoop, calls=%fused_computation.1 | loop fusion | flops 4193280 | bytes 4198400 | tf_op jit(solution)/shard_map/reduce_sum | solution.py:68
  56.5 1.2 fusion.2
  57.7 1.6 %fusion.4 = bf16[1024,2048]{1,0:T(8,128)(2,1)S(1)} fusion(bf16[1024,2048]{1,0:T(8,128)(2,1)S(1)} %copy-done.3, f32[2048]{0:T(1024)S(1)} %copy-done.6, f32[1024]{0:T(1024)S(1)} %add_rsqrt_fusion, f32[1024]{0:T(1024)S(1)} %broadcast_multiply_fusion), kind=kLoop, calls=%fused_computation.6 | loop fusion | flops 10485760 | bytes 8404992 | tf_op jit(solution)/shard_map/convert_element_type | solution.py:70
  59.4 1.4 convolution_bitcast_fusion.1
  60.8 0.5 copy-done.1
  61.3 1.5 convolution_convert_fusion.1
  62.8 3.7 %convolution_bitcast_fusion = f32[1024,1,64]{0,2,1:T(8,128)S(1)} fusion(bf16[1024,2048]{1,0:T(8,128)(2,1)} %copy-done.1, bf16[2048,64]{0,1:T(8,128)(2,1)S(1)} %copy-done), kind=kOutput, calls=%fused_computation.12 | convolution fusion | flops 268435456 | bytes 4718592 | tf_op jit(solution)/shard_map/dot_general | solution.py:97
  66.5 1.4 convolution_convert_fusion
  67.9 0.6 fusion.96
  68.6 1.3 collective-permute-start.1
  69.9 4.2 %collective-permute-start = (bf16[128,192]{0,1:T(8,128)(2,1)S(1)}, bf16[128,192]{0,1:T(8,128)(2,1)S(1)}, u32[]{:S(2)}, u32[]{:S(2)}) collective-permute-start(bf16[128,192]{0,1:T(8,128)(2,1)S(1)} %get-tuple-element.7), channel_id=1, source_target_pairs={{0,8},{8,16},{16,24},{24,32},{32,40},{40,48},{48,56},{56,64},{64,7... | collective-permute-start | bytes 147464 | tf_op jit(solution)/shard_map/ppermute | solution.py:32
  75.0 0.3 fusion.222
  75.3 0.2 fusion.87
  75.6 0.3 fusion.221
  75.9 0.2 fusion.86
  76.1 0.3 fusion.220
  76.4 0.2 fusion.85
  76.7 0.3 fusion.219
  77.0 0.2 fusion.84
  77.2 0.3 fusion.218
  77.5 0.2 fusion.83
  77.7 0.3 fusion.217
  78.0 0.2 fusion.82
  78.6 0.1 slice_add_fusion.1
  78.7 0.1 slice_add_fusion
  79.0 0.3 fusion.223
  79.3 0.2 fusion.88
  79.6 0.3 fusion.216
  79.9 0.2 fusion.81
  80.1 0.3 fusion.29
  80.5 0.4 fusion.31
  80.8 0.4 fusion.33
  81.2 0.4 fusion.35
  81.6 0.4 fusion.37
  81.9 0.4 fusion.39
  82.3 0.4 fusion.41
  82.7 0.4 fusion.98
  83.1 0.4 fusion.43
  83.4 0.7 pad_maximum_fusion
  84.3 21.6 %all_to_all.43 = bf16[64,128,32]{1,2,0:T(8,128)(2,1)S(1)} all-to-all(bf16[64,128,32]{1,2,0:T(8,128)(2,1)S(1)} %broadcast_in_dim.80), channel_id=1, replica_groups=mesh['sp'=64,'tp'=8] {'sp'}, dimensions={0} | all-to-all | bytes 1048576 | tf_op jit(solution)/shard_map/all_to_all | solution.py:59
  105.9 28.2 %all_to_all.44 = bf16[128,8,256]{0,2,1:T(8,128)(2,1)S(1)} all-to-all(bf16[128,8,256]{0,2,1:T(8,128)(2,1)S(1)} %bitcast.252), channel_id=1, replica_groups=mesh['sp'=64,'tp'=8] {'tp'}, dimensions={1} | all-to-all | bytes 1048576 | tf_op jit(solution)/shard_map/all_to_all | solution.py:162
  134.1 0.2 copy.12
  134.3 1.7 %slice_bitcast_fusion.1 = (bf16[1024,512]{0,1:T(8,128)(2,1)S(1)}, bf16[1024,512]{0,1:T(8,128)(2,1)S(1)}) fusion(bf16[512,2048]{1,0:T(8,128)(2,1)} %all-gather.2.cloned.1.call-done), kind=kLoop, calls=%fused_computation.65 | loop fusion | bytes 4194304 | tf_op jit(solution)/shard_map/transpose | solution.py:46
  136.0 0.8 fusion.9
  136.8 12.8 %all_to_all.45 = bf16[8,128,256]{2,1,0:T(8,128)(2,1)S(1)} all-to-all(bf16[8,128,256]{2,1,0:T(8,128)(2,1)S(1)} %bitcast.256), channel_id=1, replica_groups=mesh['sp'=64,'tp'=8] {'tp'}, dimensions={0} | all-to-all | bytes 1048576 | tf_op jit(solution)/shard_map/all_to_all | solution.py:166
  149.6 0.8 copy.14
  (75 shorter events, 1.0 us)
Async XLA Ops:
  6.5 56.2 %copy-start = (bf16[2048,64]{0,1:T(8,128)(2,1)S(1)}, bf16[2048,64]{0,1:T(8,128)(2,1)}, u32[]{:S(2)}) copy-start(bf16[2048,64]{0,1:T(8,128)(2,1)} %param.11) | copy-start | bytes 786436
  6.5 127.8 %all-gather.2.cloned.1.call-start = ((), (), s32[]{:S(2)}) async-start(), calls=%async_computation.3 | async-start | bytes 2359296 | tf_op jit(solution)/shard_map/all_gather | solution.py:43
  6.6 49.9 %copy-start.3 = (bf16[1024,2048]{1,0:T(8,128)(2,1)S(1)}, bf16[1024,2048]{1,0:T(8,128)(2,1)}, u32[]{:S(2)}) copy-start(bf16[1024,2048]{1,0:T(8,128)(2,1)} %param.9) | copy-start | bytes 12582916
  53.6 4.1 %copy-start.6 = (f32[2048]{0:T(1024)S(1)}, f32[2048]{0:T(1024)}, u32[]{:S(2)}) copy-start(f32[2048]{0:T(1024)} %param.10) | copy-start | bytes 24580
  59.3 1.9 %copy-start.1 = (bf16[1024,2048]{1,0:T(8,128)(2,1)}, bf16[1024,2048]{1,0:T(8,128)(2,1)S(1)}, u32[]{:S(2)}) copy-start(bf16[1024,2048]{1,0:T(8,128)(2,1)S(1)} %fusion.4) | copy-start | bytes 12582916
  61.3 5.2 %copy-start.4 = (bf16[2048,64]{0,1:T(8,128)(2,1)S(1)}, bf16[2048,64]{0,1:T(8,128)(2,1)}, u32[]{:S(2)}) copy-start(bf16[2048,64]{0,1:T(8,128)(2,1)} %param.14) | copy-start | bytes 786436
  62.7 3.8 %copy-start.2 = (bf16[1024,2048]{1,0:T(8,128)(2,1)S(1)}, bf16[1024,2048]{1,0:T(8,128)(2,1)}, u32[]{:S(2)}) copy-start(bf16[1024,2048]{1,0:T(8,128)(2,1)} %copy-done.1) | copy-start | bytes 12582916
  68.6 9.7 %collective-permute-start.1 = (bf16[128,192]{0,1:T(8,128)(2,1)S(1)}, bf16[128,192]{0,1:T(8,128)(2,1)S(1)}, u32[]{:S(2)}, u32[]{:S(2)}) collective-permute-start(bf16[128,192]{0,1:T(8,128)(2,1)S(1)} %get-tuple-element.8), channel_id=1, source_target_pairs={{8,0},{16,8},{24,16},{32,24},{40,32},{48,40},{56,48},{64,56},{72,6... | collective-permute-start | bytes 147464 | tf_op jit(solution)/shard_map/ppermute | solution.py:35
  69.9 8.5 %collective-permute-start = (bf16[128,192]{0,1:T(8,128)(2,1)S(1)}, bf16[128,192]{0,1:T(8,128)(2,1)S(1)}, u32[]{:S(2)}, u32[]{:S(2)}) collective-permute-start(bf16[128,192]{0,1:T(8,128)(2,1)S(1)} %get-tuple-element.7), channel_id=1, source_target_pairs={{0,8},{8,16},{16,24},{24,32},{32,40},{40,48},{48,56},{56,64},{64,7... | collective-permute-start | bytes 147464 | tf_op jit(solution)/shard_map/ppermute | solution.py:32
  80.1 2.5 %copy-start.7 = (f32[64]{0:T(128)S(1)}, f32[64]{0:T(128)}, u32[]{:S(2)}) copy-start(f32[64]{0:T(128)} %param.16) | copy-start | bytes 772
  81.2 3.0 %copy-start.5 = (bf16[128,32]{0,1:T(8,128)(2,1)S(1)}, bf16[128,32]{0,1:T(8,128)(2,1)}, u32[]{:S(2)}) copy-start(bf16[128,32]{0,1:T(8,128)(2,1)} %param.17) | copy-start | bytes 24580
Sparse Core Ops, SparseCore 0:
  84.3 39.5 all-gather.1
where the time goes:
time: 158 us; the launch traced here: 157 us
  blocking collectives  109 us (69%)
  between operations  14.6 us (9%)
  matrix products  13.8 us (9%)
  other arithmetic  10.3 us (7%)
  starting transfers between devices  5.46 us (3%)
  local copies, waits for them, and re-layouts  4.48 us (3%)
    all_gather x1, blocking collectives, in_one_piece(): lax.all_gather(both, axis, axis=dim, tiled=True)  46 us
    all_to_all x1, blocking collectives, body(): lax.all_to_all(own_rows, 'tp', split_axis=1, concat_axis=0, tiled=True)  28.2 us
    all_to_all x1, blocking collectives, from_everyone(): lax.all_to_all(jnp.broadcast_to(x[None], (peers, *x.shape)), axis, 0, 0,...  21.6 us
    all_to_all x1, blocking collectives, body(): lax.all_to_all(partial_cols, 'tp', split_axis=0, concat_axis=1, tiled=True)  12.8 us
    ppermute x1, starting transfers between devices, extended(): lax.ppermute(lax.slice_in_dim(block, block.shape[dim] - width, None, axis...  4.17 us
    dot_general x1, matrix products, body(): jnp.dot(normed, w_query, preferred_element_type=jnp.float32)  3.73 us
  transfers between devices with their start and end apart: 3, of which 0 were waited for; matrix products, arithmetic and copies ran while one was open for 2% of the time, Pallas kernels for 0%

commit v1 on v0

v1 whole, which is shorter than its diff:
```python
import functools

import jax
import jax.numpy as jnp
import numpy as np
from jax import lax
from jax.experimental import pallas as pl
from jax.experimental.pallas import tpu as pltpu
from jax.sharding import PartitionSpec as P

HEAD = 64
WINDOW = 128
QB = 128
NEG_BIG = -1e30
EDGE = 16
RING = 8
ORDER = (1, 7, 2, 6, 3, 5, 4)
MESH = pl.DeviceIdType.MESH
F32 = jnp.float32
BF16 = jnp.bfloat16


def angle_tables(n_sp, rows):
    half = HEAD // 2
    inverse = 10000.0 ** (-np.arange(half, dtype=np.float64) / half)

    def pair(positions):
        angles = positions[:, None].astype(np.float64) * inverse[None, :]
        cosine, sine = np.cos(angles), np.sin(angles)
        ones = np.ones((len(positions), HEAD))
        c = np.concatenate([cosine, cosine, ones], axis=1)
        s = np.concatenate([-sine, sine, 0.0 * ones], axis=1)
        return c.astype(np.float32), s.astype(np.float32)

    c, s = pair(np.arange(n_sp) * rows)
    start = np.zeros((n_sp, 8, 2 * HEAD), np.float32)
    start[:, 0], start[:, 1] = c, s
    return start, np.stack(pair(np.arange(rows)))


def kernel(
    rows,
    tokens,
    gain,
    w_query,
    w_key,
    w_value,
    w_pool,
    small,
    w_out,
    start_angles,
    row_angles,
    out,
    tok,
    gain_v,
    wq_v,
    wp_v,
    wk_v,
    wv_v,
    wo_v,
    small_v,
    start_v,
    angles_v,
    wqp,
    kvbuf,
    wkv,
    wbuf,
    q_v,
    p_ext,
    pool_v,
    kv_ext,
    mix_send,
    mix_recv,
    load_sem,
    tok_sem,
    kv1_s,
    kv1_r,
    kv2_s,
    kv2_r,
    kvd_s,
    kvd_r,
    w1_s,
    w1_r,
    w2_s,
    w2_r,
    w3_s,
    w3_r,
    wd_s,
    wd_r,
    ph_s,
    ph_r,
    kh_s,
    kh_r,
    mx_s,
    mx_r,
):
    s = lax.axis_index("sp")
    t = lax.axis_index("tp")
    n_sp = lax.axis_size("sp")
    n_tp = lax.axis_size("tp")
    x, c = t // 2, t % 2
    z, y = s // RING, s % RING
    a = y + c * (z - y)
    b = z + c * (y - z)
    step_a = 1 + (RING - 1) * c
    step_b = RING - (RING - 1) * c
    other = t + 1 - 2 * c

    def along_a(k):
        return (s + ((a + k) % RING - a) * step_a, t)

    def along_b(k):
        return (s + ((b + k) % RING - b) * step_b, t)

    def along_x(k):
        return (s, ((x + k) % 4) * 2 + c)

    def along_tp(k):
        return (s, (t + k) % n_tp)

    after = ((s + 1) % n_sp, t)
    before = ((s + n_sp - 1) % n_sp, t)

    barrier = pltpu.get_barrier_semaphore()
    peers = (
        [along_a(k) for k in range(1, RING)]
        + [along_b(k) for k in range(1, RING)]
        + [along_tp(k) for k in range(1, n_tp)]
        + [after, before]
    )
    for peer in peers:
        pl.semaphore_signal(barrier, inc=1, device_id=peer, device_id_type=MESH)

    def remote(src, dst, ssem, rsem, device):
        return pltpu.make_async_remote_copy(
            src_ref=src, dst_ref=dst, send_sem=ssem, recv_sem=rsem,
            device_id=device, device_id_type=MESH,
        )

    loads = [
        pltpu.make_async_copy(src, dst, load_sem.at[i])
        for i, (src, dst) in enumerate((
            (w_key, wk_v), (w_value, wv_v), (w_out, wo_v), (gain, gain_v),
            (small, small_v), (start_angles.at[s], start_v),
            (w_query, wq_v), (w_pool, wp_v), (row_angles, angles_v),
        ))
    ]
    blocks = rows // QB
    tok_loads = [
        pltpu.make_async_copy(
            tokens.at[pl.ds(i * QB, QB)], tok.at[pl.ds(i * QB, QB)], tok_sem.at[i]
        )
        for i in range(blocks)
    ]
    for load in loads[:6]:
        load.start()
    for load in tok_loads:
        load.start()
    for load in loads[6:]:
        load.start()
    for load in loads[:6]:
        load.wait()

    lane = lax.broadcasted_iota(jnp.int32, (1, 2 * HEAD), 1)

    def swap_halves(value):
        return pltpu.roll(value, HEAD, 1)

    wk_f, wv_f = wk_v[...].astype(F32), wv_v[...].astype(F32)
    low_head = t < n_tp // 2
    k_part = jnp.where(low_head, wk_f, swap_halves(wk_f))
    v_part = jnp.where(low_head, swap_halves(wv_f), wv_f)
    kv_piece = jnp.where(lane < HEAD, k_part, v_part)
    half_rows = kv_piece.shape[0] // 2
    kvbuf[c, b, a] = jnp.where(c == 0, kv_piece[:half_rows], kv_piece[half_rows:]).astype(BF16)
    width = wo_v.shape[1]
    unit = (
        lax.broadcasted_iota(jnp.int32, (width, width), 0)
        == lax.broadcasted_iota(jnp.int32, (width, width), 1)
    ).astype(BF16)
    wbuf[c, b, a, x] = lax.dot_general(
        unit, wo_v[...], (((1,), (1,)), ((), ())), preferred_element_type=F32
    ).astype(BF16)

    features = tok.shape[1]
    chunk = 16

    def norm_block(first, count):
        def norm_rows(i, carry):
            at = pl.ds(pl.multiple_of(first + i * chunk, chunk), chunk)
            values = tok[at, :].astype(F32)
            center = jnp.sum(values, axis=-1, keepdims=True) * (1.0 / features)
            shifted = values - center
            spread = jnp.sum(shifted * shifted, axis=-1, keepdims=True) * (1.0 / features)
            tok[at, :] = (shifted * lax.rsqrt(spread + 1e-06) * gain_v[...]).astype(BF16)
            return carry

        lax.fori_loop(0, count // chunk, norm_rows, 0, unroll=2)

    def norm_blocks(lo, hi):
        for i in range(lo, hi):
            tok_loads[i].wait()
        norm_block(lo * QB, (hi - lo) * QB)

    norm_blocks(0, 2)

    pl.semaphore_wait(barrier, len(peers))
    own_kv = kvbuf.at[c, b, a]
    kv1 = [remote(own_kv, own_kv, kv1_s.at[k], kv1_r.at[k], along_a(k)) for k in range(1, RING)]
    for k in ORDER:
        kv1[k - 1].start()
    own_w = wbuf.at[c, b, a, x]
    w1 = [remote(own_w, own_w, w1_s.at[k], w1_r.at[k], along_x(k)) for k in range(1, 4)]
    for copy in w1:
        copy.start()

    norm_blocks(2, blocks)

    def arrived(dst, ssem, rsem):
        remote(dst, dst, ssem, rsem, (s, other)).wait_recv()

    for k in range(1, 4):
        arrived(wbuf.at[c, b, a, (x + 4 - k) % 4], w1_s.at[k], w1_r.at[k])
    row_w = wbuf.at[c, b, a]
    w2 = [remote(row_w, row_w, w2_s.at[k], w2_r.at[k], along_a(k)) for k in range(1, RING)]
    for k in ORDER:
        w2[k - 1].start()

    for load in loads[6:]:
        load.wait()

    def merge_rows(i, carry):
        at = pl.ds(pl.multiple_of(i * 256, 256), 256)
        wqp[at, :] = jnp.concatenate([wq_v[at, :], wp_v[at, :]], axis=1)
        return carry

    lax.fori_loop(0, features // 256, merge_rows, 0)

    def rotated(value, first):
        at = pl.ds(first, QB)
        row_c, row_s = angles_v[0, at, :], angles_v[1, at, :]
        base_c, base_s = start_v[0:1, :], start_v[1:2, :]
        cosine = base_c * row_c - base_s * row_s
        sine = base_s * row_c + base_c * row_s
        partner = jnp.where(
            lane < HEAD // 2,
            pltpu.roll(value, 2 * HEAD - HEAD // 2, 1),
            pltpu.roll(value, HEAD // 2, 1),
        )
        return value * cosine + partner * sine

    def query_block(i, carry):
        first = pl.multiple_of(i * QB, QB)
        value = jnp.dot(tok[pl.ds(first, QB), :], wqp[...], preferred_element_type=F32)
        p_ext[pl.ds(pl.multiple_of(EDGE + first, EDGE), QB), :] = value.astype(BF16)
        turned = rotated(value, first)
        q_v[pl.ds(first, QB), :] = jnp.where(lane < HEAD, turned, 0.0).astype(BF16)
        return carry

    lax.fori_loop(0, blocks, query_block, 0)

    low_edge, high_edge = p_ext.at[pl.ds(EDGE, EDGE)], p_ext.at[pl.ds(rows, EDGE)]
    ph = [
        remote(high_edge, p_ext.at[pl.ds(0, EDGE)], ph_s.at[0], ph_r.at[0], after),
        remote(low_edge, p_ext.at[pl.ds(EDGE + rows, EDGE)], ph_s.at[1], ph_r.at[1], before),
    ]
    for k in ORDER:
        arrived(kvbuf.at[c, b, (a + RING - k) % RING], kv1_s.at[k], kv1_r.at[k])
    line_kv = kvbuf.at[c, b]
    kv2 = [remote(line_kv, line_kv, kv2_s.at[k], kv2_r.at[k], along_b(k)) for k in range(1, RING)]
    for k in ORDER:
        kv2[k - 1].start()
    kvd = []
    for k in range(RING):
        part = kvbuf.at[c, (b + RING - k) % RING]
        kvd.append(remote(part, part, kvd_s.at[k], kvd_r.at[k], (s, other)))
    kvd[0].start()
    for copy in ph:
        copy.start()
    ph[0].wait_recv()
    ph[1].wait_recv()

    seq_total = n_sp * rows
    reach = 1 + (t // 2 > 0) + 2 * (t // 2 > 1) + 4 * (t // 2 > 2)
    span = QB + 2 * EDGE
    place = lax.broadcasted_iota(jnp.int32, (QB, span), 1) - EDGE
    apart = place - lax.broadcasted_iota(jnp.int32, (QB, span), 0)
    near = (apart >= -reach) & (apart < reach)
    row_id = lax.broadcasted_iota(jnp.int32, (QB, 1), 0)
    scale = small_v[0:1, :]
    sink = small_v[1:2, 0:1]

    def pool_block(i, carry):
        first = pl.multiple_of(i * QB, QB)
        inside = place + (s * rows + first)
        band = jnp.where(near & (inside >= 0) & (inside < seq_total), 1.0, 0.0).astype(BF16)
        sums = jnp.dot(band, p_ext[pl.ds(first, span), :], preferred_element_type=F32)
        position = row_id + (s * rows + first)
        counted = (
            jnp.minimum(position + reach, seq_total) - jnp.maximum(position - reach, 0)
        ).astype(F32)
        here = p_ext[pl.ds(pl.multiple_of(EDGE + first, EDGE), QB), :].astype(F32)
        pooled = (sums / counted - here) * scale
        pool_v[pl.ds(first, QB), :] = swap_halves(pooled).astype(BF16)
        return carry

    lax.fori_loop(0, blocks, pool_block, 0)

    for k in ORDER:
        arrived(wbuf.at[c, b, (a + RING - k) % RING], w2_s.at[k], w2_r.at[k])
    line_w = wbuf.at[c, b]
    w3 = [remote(line_w, line_w, w3_s.at[k], w3_r.at[k], along_b(k)) for k in range(1, RING)]
    wd = []
    for k in range(RING):
        part = wbuf.at[c, (b + RING - k) % RING]
        wd.append(remote(part, part, wd_s.at[k], wd_r.at[k], (s, other)))

    for k in ORDER:
        arrived(kvbuf.at[c, (b + RING - k) % RING], kv2_s.at[k], kv2_r.at[k])
        kvd[k].start()
    for k in ORDER:
        w3[k - 1].start()
    for k in (0, *ORDER):
        arrived(kvbuf.at[1 - c, (a + RING - k) % RING], kvd_s.at[k], kvd_r.at[k])
    wd[0].start()

    def join_rows(i, carry):
        for j in range(RING):
            at = pl.multiple_of((i * RING + j) * 2 * half_rows, 2 * half_rows)
            wkv[pl.ds(at, half_rows), :] = kvbuf[0, i, j]
            wkv[pl.ds(pl.multiple_of(at + half_rows, half_rows), half_rows), :] = kvbuf[1, j, i]
        return carry

    lax.fori_loop(0, RING, join_rows, 0)

    def key_block(i, carry):
        first = pl.multiple_of(i * QB, QB)
        value = jnp.dot(tok[pl.ds(first, QB), :], wkv[...], preferred_element_type=F32)
        kv_ext[pl.ds(pl.multiple_of(WINDOW + first, QB), QB), :] = rotated(value, first).astype(BF16)
        return carry

    key_block(0, 0)
    key_block(blocks - 1, 0)
    key_block(1, 0)
    kh = [
        remote(
            kv_ext.at[pl.ds(rows, WINDOW)], kv_ext.at[pl.ds(0, WINDOW)],
            kh_s.at[0], kh_r.at[0], after,
        ),
        remote(
            kv_ext.at[pl.ds(WINDOW, WINDOW)], kv_ext.at[pl.ds(WINDOW + rows, WINDOW)],
            kh_s.at[1], kh_r.at[1], before,
        ),
    ]
    for copy in kh:
        copy.start()
    lax.fori_loop(2, blocks - 1, key_block, 0)

    query_at = lax.broadcasted_iota(jnp.int32, (QB, QB), 0)
    key_at = lax.broadcasted_iota(jnp.int32, (QB, QB), 1)

    def attend(i):
        first = pl.multiple_of(i * QB, QB)
        keys = kv_ext[pl.ds(first, QB + 2 * WINDOW), :]
        scores = lax.dot_general(
            q_v[pl.ds(first, QB), :], keys, (((1,), (1,)), ((), ())), preferred_element_type=F32
        ) * HEAD ** (-0.5)
        begin = s * rows + first
        low_ok = (key_at >= query_at) & (key_at + (begin - WINDOW) >= 0)
        high_ok = (key_at <= query_at) & (key_at + (begin + QB) < seq_total)
        scores = jnp.concatenate(
            [
                jnp.where(low_ok, scores[:, :QB], NEG_BIG),
                scores[:, QB : 2 * QB],
                jnp.where(high_ok, scores[:, 2 * QB :], NEG_BIG),
            ],
            axis=1,
        )
        highest = jnp.maximum(jnp.max(scores, axis=-1, keepdims=True), sink)
        expo = jnp.exp(scores - highest)
        total = jnp.sum(expo, axis=-1, keepdims=True) + jnp.exp(sink - highest)
        weights = (expo * (1.0 / total)).astype(BF16)
        result = jnp.dot(weights, keys, preferred_element_type=F32)
        mix_send[i] = jnp.where(lane < HEAD, pool_v[pl.ds(first, QB), :].astype(F32), result).astype(BF16)

    def mix_copy(i):
        return remote(mix_send.at[i], mix_recv.at[t], mx_s.at[i], mx_r.at[t], (s, i))

    def hand_over(i):
        @pl.when(i != t)
        def _():
            mix_copy(i).start()

        @pl.when(i == t)
        def _():
            mix_recv[i] = mix_send[i]

    def inner(i, carry):
        attend(i)
        hand_over(i)
        return carry

    lax.fori_loop(1, blocks - 1, inner, 0)
    kh[0].wait_recv()
    attend(0)
    hand_over(0)
    kh[1].wait_recv()
    attend(blocks - 1)
    hand_over(blocks - 1)

    for k in ORDER:
        arrived(wbuf.at[c, (b + RING - k) % RING], w3_s.at[k], w3_r.at[k])
        wd[k].start()

    for k in range(1, n_tp):
        source = (t + k) % n_tp
        remote(mix_recv.at[source], mix_recv.at[source], mx_s.at[source], mx_r.at[source], (s, other)).wait_recv()
    left, right = [], []
    for j in range(n_tp // 2):
        even, odd = mix_recv[2 * j].astype(F32), mix_recv[2 * j + 1].astype(F32)
        left.append(jnp.where(lane < HEAD, swap_halves(even), odd).astype(BF16))
        right.append(jnp.where(lane < HEAD, even, swap_halves(odd)).astype(BF16))
    mixed = jnp.concatenate(left + right, axis=1)

    for k in (0, *ORDER):
        arrived(wbuf.at[1 - c, (a + RING - k) % RING], wd_s.at[k], wd_r.at[k])

    span_out = RING * width
    for i in range(RING):
        parts = []
        for j in range(4):
            parts.append(wbuf[0, i, :, j].reshape(span_out, QB))
            parts.append(wbuf[1, :, i, j].reshape(span_out, QB))
        out[:, i * span_out : (i + 1) * span_out] = lax.dot_general(
            mixed, jnp.concatenate(parts, axis=1), (((1,), (1,)), ((), ())),
            preferred_element_type=F32,
        ).astype(BF16)

    for copy in (*kv1, *kv2, *kvd, *w1, *w2, *w3, *wd, *ph, *kh):
        copy.wait_send()
    for i in range(blocks):
        @pl.when(i != t)
        def _():
            mix_copy(i).wait_send()


def body(tokens, norm_gain, w_query, w_key, w_value, w_pool_in, sink_logit, pool_scale, w_out):
    rows, features = tokens.shape
    n_sp, n_tp = lax.axis_size("sp"), lax.axis_size("tp")
    start, row = angle_tables(n_sp, rows)
    small = jnp.concatenate(
        [
            jnp.pad(pool_scale[None, :], ((0, 0), (HEAD, 0))),
            jnp.broadcast_to(sink_logit[:, None], (7, 2 * HEAD)),
        ],
        axis=0,
    )
    dma, vmem = pltpu.SemaphoreType.DMA, pltpu.VMEM
    half = w_key.shape[0] // 2
    width = w_out.shape[1]
    pair = 2 * HEAD
    scratch = [
        vmem((rows, features), BF16),
        vmem((1, features), F32),
        vmem(w_query.shape, BF16),
        vmem(w_pool_in.shape, BF16),
        vmem(w_key.shape, BF16),
        vmem(w_value.shape, BF16),
        vmem(w_out.shape, BF16),
        vmem((8, pair), F32),
        vmem((8, pair), F32),
        vmem((2, rows, pair), F32),
        vmem((features, pair), BF16),
        vmem((2, RING, RING, half, pair), BF16),
        vmem((features, pair), BF16),
        vmem((2, RING, RING, n_tp // 2, width, w_out.shape[0]), BF16),
        vmem((rows, pair), BF16),
        vmem((rows + 2 * EDGE, pair), BF16),
        vmem((rows, pair), BF16),
        vmem((rows + 2 * WINDOW, pair), BF16),
        vmem((n_tp, QB, pair), BF16),
        vmem((n_tp, QB, pair), BF16),
        dma((9,)),
        dma((rows // QB,)),
    ]
    counts = (8, 8, 8, 8, 8, 8, 4, 4, 8, 8, 8, 8, 8, 8, 2, 2, 2, 2, 8, 8)
    scratch += [dma((n,)) for n in counts]
    return pl.pallas_call(
        functools.partial(kernel, rows),
        name="mixer",
        out_shape=jax.ShapeDtypeStruct((rows // n_tp, w_out.shape[1] * n_sp), BF16),
        in_specs=[pl.BlockSpec(memory_space=pl.ANY)] * 10,
        out_specs=pl.BlockSpec(memory_space=pltpu.VMEM),
        scratch_shapes=scratch,
        compiler_params=pltpu.CompilerParams(
            collective_id=0, has_side_effects=True, vmem_limit_bytes=60 * 2**20
        ),
    )(
        tokens, norm_gain[None, :], w_query, w_key, w_value, w_pool_in, small, w_out,
        jnp.asarray(start), jnp.asarray(row),
    )


def solution(mesh):
    in_specs = (
        P("sp", None),
        P(),
        P(None, "tp"),
        P("sp", None),
        P("sp", None),
        P(None, "tp"),
        P("tp"),
        P("tp"),
        P("tp", "sp"),
    )
    out_specs = P(("sp", "tp"), None)
    return jax.shard_map(body, mesh=mesh, in_specs=in_specs, out_specs=out_specs, check_vma=False)
```

time: 158 us -> 77.7 us (0.49)
  the two profiles are of different devices: /device:TPU:1 before, /device:TPU:8 now
where the time goes in v1:
time: 77.7 us; the launch traced here: 77.4 us
  Pallas kernels  68.2 us (88%)
  local copies, waits for them, and re-layouts  7.18 us (9%)
  other arithmetic  1.32 us (2%)
    pallas_call x1, Pallas kernels, body(): pl.pallas_call(functools.partial(kernel, rows), name='mixer', out_shape=j...  68.2 us
    unnamed x4, local copies, waits for them, and re-layouts  7.18 us

profile of v1, /device:TPU:8, one launch (start us, length us, event | category | flops | bytes accessed | tf_op | source)
XLA Modules:
  0.0 77.4 jit_solution(10221238114958356379)
XLA Ops:
  0.7 1.3 %pad_select_fusion.small = f32[8,128]{1,0:T(8,128)} fusion(f32[1,64]{1,0:T(1,128)} %bitcast.5, f32[]{:T(128)} %bitcast.3), kind=kLoop, calls=%fused_computation.1 | loop fusion | flops 2048 | bytes 4356 | tf_op jit(solution)/shard_map/concatenate | solution.py:451
  2.0 1.4 %copy.14.w_out = bf16[128,32]{1,0:T(8,128)(2,1)} copy(bf16[128,32]{0,1:T(8,128)(2,1)} %param.19) | data formatting | bytes 16384 | tf_op args[8]
  3.4 2.0 %copy.12.w_query = bf16[2048,64]{1,0:T(8,128)(2,1)} copy(bf16[2048,64]{0,1:T(8,128)(2,1)} %param.13) | data formatting | bytes 524288 | tf_op args[2]
  5.3 1.9 %copy.13.w_pool = bf16[2048,64]{1,0:T(8,128)(2,1)} copy(bf16[2048,64]{0,1:T(8,128)(2,1)} %param.16) | data formatting | bytes 524288 | tf_op args[5]
  7.3 68.2 %mixer.1 = bf16[128,2048]{1,0:T(8,128)(2,1)} custom-call(bf16[1024,2048]{1,0:T(8,128)(2,1)} %tokens.1, f32[1,2048]{1,0:T(1,128)} %bitcast.4, bf16[2048,64]{1,0:T(8,128)(2,1)} %copy.12.w_query, bf16[32,128]{1,0:T(8,128)(2,1)} %w_key.1, bf16[32,128]{1,0:T(8,128)(2,1)} %w_value.1, bf16[2048,64]{1,0:T(8,128)(2,1)} %copy.13.w_pool, ...), custom_call_target="tpu_custom_call" | custom-call | tf_op jit(solution)/shard_map/mixer/pallas_call | solution.py:488
  75.5 1.9 %copy.17 = bf16[128,2048]{1,0:T(8,128)(2,1)} copy(bf16[128,2048]{1,0:T(8,128)(2,1)} %mixer.1) | data formatting | bytes 1048576

commit v2 on v1

v2 whole, which is shorter than its diff:
```python
import functools

import jax
import jax.numpy as jnp
import numpy as np
from jax import lax
from jax.experimental import pallas as pl
from jax.experimental.pallas import tpu as pltpu
from jax.sharding import PartitionSpec as P

HEAD = 64
WINDOW = 128
QB = 128
NEG_BIG = -1e30
EDGE = 16
RING = 8
ORDER = (1, 7, 2, 6, 3, 5, 4)
MESH = pl.DeviceIdType.MESH
F32 = jnp.float32
BF16 = jnp.bfloat16


def angle_tables(n_sp, rows):
    half = HEAD // 2
    inverse = np.float32(10000.0) ** (-np.arange(half, dtype=np.float32) / np.float32(half))

    def pair(positions):
        angles = positions[:, None].astype(np.float64) * inverse[None, :].astype(np.float64)
        cosine, sine = np.cos(angles), np.sin(angles)
        ones = np.ones((len(positions), HEAD))
        c = np.concatenate([cosine, cosine, ones], axis=1)
        s = np.concatenate([-sine, sine, 0.0 * ones], axis=1)
        return c.astype(np.float32), s.astype(np.float32)

    def cut(value):
        scale = np.exp2(np.floor(np.log2(np.where(value == 0, 1.0, np.abs(value)))) - 7)
        return np.trunc(value / scale) * scale

    exact = inverse.astype(np.float64)
    pieces = [cut(exact)]
    pieces.append(cut(exact - pieces[0]))
    pieces.append(exact - pieces[0] - pieces[1])
    start = np.zeros((n_sp, 8, 2 * HEAD), np.float32)
    start[:, 0], start[:, 1] = pair(np.arange(n_sp) * rows)
    start[:, 2, :half], start[:, 2, half:HEAD] = -1.0, 1.0
    for row, value in zip(range(3, 7), (*pieces, exact)):
        start[:, row, :HEAD] = np.concatenate([value, value])
    return start, np.stack(pair(np.arange(rows)))


def kernel(
    rows,
    tokens,
    gain,
    w_query,
    w_key,
    w_value,
    w_pool,
    scale,
    sink,
    w_out,
    start_angles,
    row_angles,
    out,
    tok,
    nrm,
    gain_v,
    wk_v,
    wv_v,
    scale_v,
    sink_v,
    start_v,
    angles_v,
    wqp,
    kvbuf,
    wkv,
    wbuf,
    q_v,
    p_ext,
    pool_v,
    kv_ext,
    mix_send,
    mix_recv,
    load_sem,
    tok_sem,
    kv1_s,
    kv1_r,
    kv2_s,
    kv2_r,
    kvd_s,
    kvd_r,
    w1_s,
    w1_r,
    w2_s,
    w2_r,
    w3_s,
    w3_r,
    wd_s,
    wd_r,
    ph_s,
    ph_r,
    kh_s,
    kh_r,
    mx_s,
    mx_r,
):
    s = lax.axis_index("sp")
    t = lax.axis_index("tp")
    n_sp = lax.axis_size("sp")
    n_tp = lax.axis_size("tp")
    x, c = t // 2, t % 2
    z, y = s // RING, s % RING
    a = y + c * (z - y)
    b = z + c * (y - z)
    step_a = 1 + (RING - 1) * c
    step_b = RING - (RING - 1) * c
    other = t + 1 - 2 * c

    def along_a(k):
        return (s + ((a + k) % RING - a) * step_a, t)

    def along_b(k):
        return (s + ((b + k) % RING - b) * step_b, t)

    def along_x(k):
        return (s, ((x + k) % 4) * 2 + c)

    def along_tp(k):
        return (s, (t + k) % n_tp)

    after = ((s + 1) % n_sp, t)
    before = ((s + n_sp - 1) % n_sp, t)

    barrier = pltpu.get_barrier_semaphore()
    peers = (
        [along_a(k) for k in range(1, RING)]
        + [along_b(k) for k in range(1, RING)]
        + [along_tp(k) for k in range(1, n_tp)]
        + [after, before]
    )
    for peer in peers:
        pl.semaphore_signal(barrier, inc=1, device_id=peer, device_id_type=MESH)

    def remote(src, dst, ssem, rsem, device):
        return pltpu.make_async_remote_copy(
            src_ref=src, dst_ref=dst, send_sem=ssem, recv_sem=rsem,
            device_id=device, device_id_type=MESH,
        )

    loads = [
        pltpu.make_async_copy(src, dst, load_sem.at[i])
        for i, (src, dst) in enumerate((
            (w_key, wk_v), (w_value, wv_v), (w_out, wbuf.at[c, b, a, x]), (gain, gain_v),
            (w_query, wqp.at[pl.ds(0, HEAD)]), (w_pool, wqp.at[pl.ds(HEAD, HEAD)]),
            (row_angles, angles_v), (start_angles.at[s], start_v), (scale, scale_v), (sink, sink_v),
        ))
    ]
    blocks = rows // QB
    tok_loads = [
        pltpu.make_async_copy(
            tokens.at[pl.ds(i * QB, QB)], tok.at[pl.ds(i * QB, QB)], tok_sem.at[i]
        )
        for i in range(blocks)
    ]
    for load in loads[:3]:
        load.start()
    for load in tok_loads:
        load.start()
    for load in loads[3:]:
        load.start()
    with jax.named_scope("load_wait"):
        for load in loads[:3]:
            load.wait()

    lane = lax.broadcasted_iota(jnp.int32, (1, 2 * HEAD), 1)

    def swap_halves(value):
        return pltpu.roll(value, HEAD, 1)

    wk_f, wv_f = wk_v[...].astype(F32), wv_v[...].astype(F32)
    low_head = t < n_tp // 2
    k_part = jnp.where(low_head, wk_f, swap_halves(wk_f))
    v_part = jnp.where(low_head, swap_halves(wv_f), wv_f)
    kv_piece = jnp.where(lane < HEAD, k_part, v_part)
    half_rows = kv_piece.shape[0] // 2
    kvbuf[c, b, a] = jnp.where(c == 0, kv_piece[:half_rows], kv_piece[half_rows:]).astype(BF16)
    width = wbuf.shape[4]

    with jax.named_scope("barrier_wait"):
        pl.semaphore_wait(barrier, len(peers))

    own_w = wbuf.at[c, b, a, x]
    w1 = [remote(own_w, own_w, w1_s.at[k], w1_r.at[k], along_x(k)) for k in range(1, 4)]
    for copy in w1:
        copy.start()
    own_kv = kvbuf.at[c, b, a]
    kv1 = [remote(own_kv, own_kv, kv1_s.at[k], kv1_r.at[k], along_a(k)) for k in range(1, RING)]
    for k in ORDER:
        kv1[k - 1].start()

    features = tok.shape[1]
    chunk, slab = 32, 128

    def slabs():
        return [slice(j * slab, (j + 1) * slab) for j in range(features // slab)]

    def norm_at(i):
        return pl.ds(pl.multiple_of(i * chunk, chunk), chunk)

    def norm_center(i):
        parts = [tok[norm_at(i), cols].astype(F32) for cols in slabs()]
        while len(parts) > 1:
            parts = [p + q for p, q in zip(parts[::2], parts[1::2])]
        return jnp.sum(parts[0], axis=-1, keepdims=True) * (1.0 / features)

    def norm_spread(i, center):
        total = [0.0, 0.0]
        for j, cols in enumerate(slabs()):
            shifted = tok[norm_at(i), cols].astype(F32) - center
            total[j % 2] = total[j % 2] + shifted * shifted
        spread = jnp.sum(total[0] + total[1], axis=-1, keepdims=True) * (1.0 / features)
        return lax.rsqrt(spread + 1e-06)

    def norm_store(i, center, inverse):
        for cols in slabs():
            shifted = tok[norm_at(i), cols].astype(F32) - center
            nrm[norm_at(i), cols] = (shifted * inverse * gain_v[:, cols]).astype(BF16)

    def norm_rows(lo, hi):
        def step(i, carry):
            later, center, inverse = carry
            norm_store(i, center, inverse)
            ahead = jnp.minimum(i + 1, hi - 1)
            next_inverse = norm_spread(ahead, later)
            return norm_center(jnp.minimum(i + 2, hi - 1)), later, next_inverse

        first = norm_center(lo)
        lax.fori_loop(lo, hi, step, (norm_center(lo + 1), first, norm_spread(lo, first)))

    def norm_blocks(lo, hi):
        for i in range(lo, hi):
            tok_loads[i].wait()
        norm_rows(lo * QB // chunk, hi * QB // chunk)

    def arrived(dst, ssem, rsem):
        remote(dst, dst, ssem, rsem, (s, other)).wait_recv()

    loads[3].wait()
    with jax.named_scope("norm_first"):
        norm_blocks(0, blocks // 2)
    with jax.named_scope("w1_wait"):
        for k in range(1, 4):
            arrived(wbuf.at[c, b, a, (x + 4 - k) % 4], w1_s.at[k], w1_r.at[k])
    row_w = wbuf.at[c, b, a]
    w2 = [remote(row_w, row_w, w2_s.at[k], w2_r.at[k], along_a(k)) for k in range(1, RING)]
    for k in ORDER:
        w2[k - 1].start()
    with jax.named_scope("norm_rest"):
        norm_blocks(blocks // 2, blocks)
    with jax.named_scope("kv1_wait"):
        for k in ORDER:
            arrived(kvbuf.at[c, b, (a + RING - k) % RING], kv1_s.at[k], kv1_r.at[k])
    line_kv = kvbuf.at[c, b]
    kv2 = [remote(line_kv, line_kv, kv2_s.at[k], kv2_r.at[k], along_b(k)) for k in range(1, RING)]
    for k in ORDER:
        kv2[k - 1].start()
    kvd = []
    for k in range(RING):
        part = kvbuf.at[c, (b + RING - k) % RING]
        kvd.append(remote(part, part, kvd_s.at[k], kvd_r.at[k], (s, other)))
    kvd[0].start()
    for load in loads[4:]:
        load.wait()

    seq_total = n_sp * rows
    base_c, base_s = start_v[0:1, :], start_v[1:2, :]
    signed, piece_1, piece_2, piece_3, whole = (start_v[i : i + 1, :] for i in range(2, 7))
    turn_rows = 64

    def turn_block(i, carry):
        at = pl.ds(pl.multiple_of(i * turn_rows, turn_rows), turn_rows)
        row_c, row_s = angles_v[0, at, :], angles_v[1, at, :]
        cosine = base_c * row_c - base_s * row_s
        sine = base_s * row_c + base_c * row_s
        position = (
            lax.broadcasted_iota(jnp.int32, (turn_rows, 1), 0) + (s * rows + i * turn_rows)
        ).astype(F32)
        rounding = position * whole - position * piece_1
        rounding = rounding - position * piece_2 - position * piece_3
        rounding = rounding * signed
        angles_v[0, at, :] = cosine - rounding * sine
        angles_v[1, at, :] = sine + rounding * cosine
        return carry

    with jax.named_scope("turns"):
        lax.fori_loop(0, rows // turn_rows, turn_block, 0)

    def rotated(value, at):
        partner = jnp.where(
            lane < HEAD // 2,
            pltpu.roll(value, 2 * HEAD - HEAD // 2, 1),
            pltpu.roll(value, HEAD // 2, 1),
        )
        return value * angles_v[0, at, :] + partner * angles_v[1, at, :]

    wide = 2 * QB

    def query_block(i, carry):
        at = pl.ds(pl.multiple_of(i * wide, wide), wide)
        value = lax.dot_general(
            nrm[at, :], wqp[...], (((1,), (1,)), ((), ())), preferred_element_type=F32
        )
        p_ext[pl.ds(pl.multiple_of(EDGE + i * wide, EDGE), wide), :] = value.astype(BF16)
        q_v[at, :] = jnp.where(lane < HEAD, rotated(value, at), 0.0).astype(BF16)
        return carry

    with jax.named_scope("query_proj"):
        lax.fori_loop(0, rows // wide, query_block, 0)

    low_edge, high_edge = p_ext.at[pl.ds(EDGE, EDGE)], p_ext.at[pl.ds(rows, EDGE)]
    ph = [
        remote(high_edge, p_ext.at[pl.ds(0, EDGE)], ph_s.at[0], ph_r.at[0], after),
        remote(low_edge, p_ext.at[pl.ds(EDGE + rows, EDGE)], ph_s.at[1], ph_r.at[1], before),
    ]
    for copy in ph:
        copy.start()

    with jax.named_scope("w2_wait"):
        for k in ORDER:
            arrived(wbuf.at[c, b, (a + RING - k) % RING], w2_s.at[k], w2_r.at[k])

    half_line = RING // 2

    def half_at(owner, place, u):
        return wbuf.at[owner, place, pl.ds(half_line * u, half_line)]

    def to_right(d, u):
        part = half_at(c, (b + RING - d) % RING, u)
        return remote(part, part, w3_s.at[0, 2 * d + u], w3_r.at[0, 2 * d + u], along_b(1))

    def to_left(d, u):
        part = half_at(c, (b + d) % RING, u)
        return remote(part, part, w3_s.at[1, 2 * d + u], w3_r.at[1, 2 * d + u], along_b(RING - 1))

    def across(way, d, u):
        part = half_at(c, (b + (RING - d if way == 0 else d)) % RING, u)
        index = 2 * d + u
        return remote(part, part, wd_s.at[way, index], wd_r.at[way, index], (s, other))

    ring_copies, cross_copies = [], []

    def launch(copy, into):
        copy.start()
        into.append(copy)

    for u in range(2):
        launch(to_right(0, u), ring_copies)
        launch(to_left(0, u), ring_copies)
        launch(across(u, 0, u), cross_copies)

    ring_steps = [((d, u), (d, u)) for d in (1, 2, 3) for u in (0, 1)] + [((4, 0), (4, 1))]

    def ring_advance(step):
        with jax.named_scope("ring_wait"):
            for way, (d, u) in enumerate(ring_steps[step]):
                send = to_right if way == 0 else to_left
                place = (b + (RING - d if way == 0 else d)) % RING
                index = 2 * (d - 1) + u
                arrived(half_at(c, place, u), w3_s.at[way, index], w3_r.at[way, index])
                if d < 3 or (d == 3 and u == way):
                    launch(send(d, u), ring_copies)
                launch(across(way, d, u), cross_copies)

    reach = 1 + (t // 2 > 0) + 2 * (t // 2 > 1) + 4 * (t // 2 > 2)
    span = QB + 2 * EDGE
    place = lax.broadcasted_iota(jnp.int32, (QB, span), 1) - EDGE
    apart = place - lax.broadcasted_iota(jnp.int32, (QB, span), 0)
    near = (apart >= -reach) & (apart < reach)
    row_id = lax.broadcasted_iota(jnp.int32, (QB, 1), 0)
    scales = jnp.concatenate([scale_v[...], scale_v[...]], axis=1)
    sinks = sink_v[...]

    def pool_block(i, carry):
        first = pl.multiple_of(i * QB, QB)
        inside = place + (s * rows + first)
        band = jnp.where(near & (inside >= 0) & (inside < seq_total), 1.0, 0.0).astype(BF16)
        sums = jnp.dot(band, p_ext[pl.ds(first, span), :], preferred_element_type=F32)
        position = row_id + (s * rows + first)
        counted = (
            jnp.minimum(position + reach, seq_total) - jnp.maximum(position - reach, 0)
        ).astype(F32)
        here = p_ext[pl.ds(pl.multiple_of(EDGE + first, EDGE), QB), :].astype(F32)
        pooled = (sums / counted - here) * scales
        pool_v[pl.ds(first, QB), :] = swap_halves(pooled).astype(BF16)
        return carry

    with jax.named_scope("pool_halo"):
        ph[0].wait_recv()
        ph[1].wait_recv()
    with jax.named_scope("pool_mix"):
        lax.fori_loop(0, blocks, pool_block, 0)

    with jax.named_scope("kv2_wait"):
        for k in ORDER:
            arrived(kvbuf.at[c, (b + RING - k) % RING], kv2_s.at[k], kv2_r.at[k])
            kvd[k].start()
    with jax.named_scope("kvd_wait"):
        for k in (0, *ORDER):
            arrived(kvbuf.at[1 - c, (a + RING - k) % RING], kvd_s.at[k], kvd_r.at[k])

    def join_rows(i, carry):
        for j in range(RING):
            at = pl.multiple_of((i * RING + j) * 2 * half_rows, 2 * half_rows)
            wkv[pl.ds(at, half_rows), :] = kvbuf[0, i, j]
            wkv[pl.ds(pl.multiple_of(at + half_rows, half_rows), half_rows), :] = kvbuf[1, j, i]
        return carry

    with jax.named_scope("kv_join"):
        lax.fori_loop(0, RING, join_rows, 0)

    def key_rows(first, count):
        at = pl.ds(pl.multiple_of(first, QB), count)
        value = jnp.dot(nrm[at, :], wkv[...], preferred_element_type=F32)
        kv_ext[pl.ds(pl.multiple_of(WINDOW + first, QB), count), :] = rotated(value, at).astype(BF16)

    with jax.named_scope("key_edge"):
        key_rows(0, QB)
        key_rows(rows - QB, QB)
    ring_advance(0)
    kh = [
        remote(
            kv_ext.at[pl.ds(rows, WINDOW)], kv_ext.at[pl.ds(0, WINDOW)],
            kh_s.at[0], kh_r.at[0], after,
        ),
        remote(
            kv_ext.at[pl.ds(WINDOW, WINDOW)], kv_ext.at[pl.ds(WINDOW + rows, WINDOW)],
            kh_s.at[1], kh_r.at[1], before,
        ),
    ]
    for copy in kh:
        copy.start()

    def key_wide(i, carry):
        key_rows(QB + i * wide, wide)
        return carry

    with jax.named_scope("key_rest"):
        lax.fori_loop(0, (rows - 2 * QB) // wide, key_wide, 0)
    ring_advance(1)

    query_at = lax.broadcasted_iota(jnp.int32, (QB, QB), 0)
    key_at = lax.broadcasted_iota(jnp.int32, (QB, QB), 1)

    def attend(i):
        first = pl.multiple_of(i * QB, QB)
        keys = kv_ext[pl.ds(first, QB + 2 * WINDOW), :]
        scores = lax.dot_general(
            q_v[pl.ds(first, QB), :], keys, (((1,), (1,)), ((), ())), preferred_element_type=F32
        ) * HEAD ** (-0.5)
        begin = s * rows + first
        low_ok = (key_at >= query_at) & (key_at + (begin - WINDOW) >= 0)
        high_ok = (key_at <= query_at) & (key_at + (begin + QB) < seq_total)
        scores = jnp.concatenate(
            [
                jnp.where(low_ok, scores[:, :QB], NEG_BIG),
                scores[:, QB : 2 * QB],
                jnp.where(high_ok, scores[:, 2 * QB :], NEG_BIG),
            ],
            axis=1,
        )
        highest = jnp.maximum(jnp.max(scores, axis=-1, keepdims=True), sinks)
        expo = jnp.exp(scores - highest)
        total = jnp.sum(expo, axis=-1, keepdims=True) + jnp.exp(sinks - highest)
        weights = (expo * (1.0 / total)).astype(BF16)
        result = jnp.dot(weights, keys, preferred_element_type=F32)
        mix_send[i] = jnp.where(lane < HEAD, pool_v[pl.ds(first, QB), :].astype(F32), result).astype(BF16)

    def mix_copy(i):
        return remote(mix_send.at[i], mix_recv.at[t], mx_s.at[i], mx_r.at[t], (s, i))

    def hand_over(i):
        @pl.when(i != t)
        def _():
            mix_copy(i).start()

        @pl.when(i == t)
        def _():
            mix_recv[i] = mix_send[i]

    def attend_pair(i, j):
        with jax.named_scope("attend"):
            attend(i)
            attend(j)
        hand_over(i)
        hand_over(j)

    attend_pair(1, 2)
    ring_advance(2)
    attend_pair(3, 4)
    ring_advance(3)
    attend_pair(5, 6)
    ring_advance(4)
    with jax.named_scope("key_halo"):
        kh[0].wait_recv()
        kh[1].wait_recv()
    attend_pair(0, blocks - 1)
    ring_advance(5)
    ring_advance(6)

    with jax.named_scope("mix_wait"):
        for k in range(1, n_tp):
            source = (t + k) % n_tp
            remote(mix_recv.at[source], mix_recv.at[source], mx_s.at[source], mx_r.at[source], (s, other)).wait_recv()
    left, right = [], []
    for j in range(n_tp // 2):
        even, odd = mix_recv[2 * j].astype(F32), mix_recv[2 * j + 1].astype(F32)
        left.append(jnp.where(lane < HEAD, swap_halves(even), odd).astype(BF16))
        right.append(jnp.where(lane < HEAD, even, swap_halves(odd)).astype(BF16))
    mixed = jnp.concatenate(left + right, axis=1)

    with jax.named_scope("wd_wait"):
        for way in range(2):
            place = a
            arrived(half_at(1 - c, place, way), wd_s.at[way, way], wd_r.at[way, way])
        for step in ring_steps:
            for way, (d, u) in enumerate(step):
                place = (a + (RING - d if way == 0 else d)) % RING
                index = 2 * d + u
                arrived(half_at(1 - c, place, u), wd_s.at[way, index], wd_r.at[way, index])

    span_out = RING * width
    with jax.named_scope("out_proj"):
        for i in range(RING):
            parts = []
            for j in range(4):
                parts.append(wbuf[0, i, :, j].reshape(span_out, QB))
                parts.append(wbuf[1, :, i, j].reshape(span_out, QB))
            out[:, i * span_out : (i + 1) * span_out] = lax.dot_general(
                mixed, jnp.concatenate(parts, axis=1), (((1,), (1,)), ((), ())),
                preferred_element_type=F32,
            ).astype(BF16)

    with jax.named_scope("send_wait"):
        for copy in (*kv1, *kv2, *kvd, *w1, *w2, *ring_copies, *cross_copies, *ph, *kh):
            copy.wait_send()
    for i in range(blocks):
        @pl.when(i != t)
        def _():
            mix_copy(i).wait_send()


def body(tokens, norm_gain, w_query, w_key, w_value, w_pool_in, sink_logit, pool_scale, w_out):
    rows, features = tokens.shape
    n_sp, n_tp = lax.axis_size("sp"), lax.axis_size("tp")
    start, row = angle_tables(n_sp, rows)
    dma, vmem = pltpu.SemaphoreType.DMA, pltpu.VMEM
    half = w_key.shape[0] // 2
    width = w_out.shape[1]
    pair = 2 * HEAD
    scratch = [
        vmem((rows, features), BF16),
        vmem((rows, features), BF16),
        vmem((1, features), F32),
        vmem(w_key.shape, BF16),
        vmem(w_value.shape, BF16),
        vmem((1, HEAD), F32),
        vmem((1, 1), F32),
        vmem((8, pair), F32),
        vmem((2, rows, pair), F32),
        vmem((pair, features), BF16),
        vmem((2, RING, RING, half, pair), BF16),
        vmem((features, pair), BF16),
        vmem((2, RING, RING, n_tp // 2, width, w_out.shape[0]), BF16),
        vmem((rows, pair), BF16),
        vmem((rows + 2 * EDGE, pair), BF16),
        vmem((rows, pair), BF16),
        vmem((rows + 2 * WINDOW, pair), BF16),
        vmem((n_tp, QB, pair), BF16),
        vmem((n_tp, QB, pair), BF16),
        dma((10,)),
        dma((rows // QB,)),
    ]
    counts = (8, 8, 8, 8, 8, 8, 4, 4, 8, 8, (2, 8), (2, 8), (2, 10), (2, 10), 2, 2, 2, 2, 8, 8)
    scratch += [dma(n if isinstance(n, tuple) else (n,)) for n in counts]
    return pl.pallas_call(
        functools.partial(kernel, rows),
        name="mixer",
        out_shape=jax.ShapeDtypeStruct((rows // n_tp, w_out.shape[1] * n_sp), BF16),
        in_specs=[pl.BlockSpec(memory_space=pl.ANY)] * 11,
        out_specs=pl.BlockSpec(memory_space=pltpu.VMEM),
        scratch_shapes=scratch,
        compiler_params=pltpu.CompilerParams(
            collective_id=0, has_side_effects=True, vmem_limit_bytes=60 * 2**20
        ),
    )(
        tokens, norm_gain[None, :], w_query.T, w_key, w_value, w_pool_in.T, pool_scale[None, :], sink_logit[None, :], w_out.T,
        jnp.asarray(start), jnp.asarray(row),
    )


def solution(mesh):
    in_specs = (
        P("sp", None),
        P(),
        P(None, "tp"),
        P("sp", None),
        P("sp", None),
        P(None, "tp"),
        P("tp"),
        P("tp"),
        P("tp", "sp"),
    )
    out_specs = P(("sp", "tp"), None)
    return jax.shard_map(body, mesh=mesh, in_specs=in_specs, out_specs=out_specs, check_vma=False)
```

time: 77.7 us -> 55.1 us (0.71)
  the two profiles are of different devices: /device:TPU:8 before, /device:TPU:1 now
where the time goes in v2:
time: 55.1 us; the launch traced here: 55 us
  Pallas kernels  52.4 us (95%)
  local copies, waits for them, and re-layouts  1.88 us (3%)
  between operations  0.66 us (1%)
    pallas_call x1, Pallas kernels, body(): pl.pallas_call(functools.partial(kernel, rows), name='mixer', out_shape=j...  52.4 us
    unnamed x1, local copies, waits for them, and re-layouts  1.88 us

profile of v2, /device:TPU:1, one launch (start us, length us, event | category | flops | bytes accessed | tf_op | source)
XLA Modules:
  0.0 55.0 jit_solution(6503446189184067259)
XLA Ops:
  0.7 52.4 %mixer.1 = bf16[128,2048]{1,0:T(8,128)(2,1)} custom-call(bf16[1024,2048]{1,0:T(8,128)(2,1)} %tokens.1, f32[1,2048]{1,0:T(1,128)} %bitcast.9, bf16[64,2048]{1,0:T(8,128)(2,1)} %bitcast.7, bf16[32,128]{1,0:T(8,128)(2,1)} %w_key.1, bf16[32,128]{1,0:T(8,128)(2,1)} %w_value.1, bf16[64,2048]{1,0:T(8,128)(2,1)} %bitcast.8, f32[1,64]{1,0:T(1,128)} %bitcast.11, ...), custom_call_target="tpu_custom_call" | custom-call | tf_op jit(solution)/shard_map/mixer/pallas_call | solution.py:585
  53.1 1.9 %copy.14 = bf16[128,2048]{1,0:T(8,128)(2,1)} copy(bf16[128,2048]{1,0:T(8,128)(2,1)} %mixer.1) | data formatting | bytes 1048576

commit v3 on v2

v3 whole, which is shorter than its diff:
```python
import functools

import jax
import jax.numpy as jnp
import numpy as np
from jax import lax
from jax.experimental import pallas as pl
from jax.experimental.pallas import tpu as pltpu
from jax.sharding import PartitionSpec as P

HEAD = 64
WINDOW = 128
QB = 128
NEG_BIG = -1e30
EDGE = 16
RING = 8
ORDER = (1, 7, 2, 6, 3, 5, 4)
FAR_FIRST = (4, 5, 3, 6, 2, 7, 1)
MESH = pl.DeviceIdType.MESH
F32 = jnp.float32
BF16 = jnp.bfloat16


def angle_tables(n_sp, rows):
    half = HEAD // 2
    inverse = np.float32(10000.0) ** (-np.arange(half, dtype=np.float32) / np.float32(half))

    def pair(positions):
        angles = positions[:, None].astype(np.float64) * inverse[None, :].astype(np.float64)
        cosine, sine = np.cos(angles), np.sin(angles)
        ones = np.ones((len(positions), HEAD))
        c = np.concatenate([cosine, cosine, ones], axis=1)
        s = np.concatenate([-sine, sine, 0.0 * ones], axis=1)
        return c.astype(np.float32), s.astype(np.float32)

    def cut(value):
        scale = np.exp2(np.floor(np.log2(np.where(value == 0, 1.0, np.abs(value)))) - 7)
        return np.trunc(value / scale) * scale

    exact = inverse.astype(np.float64)
    pieces = [cut(exact)]
    pieces.append(cut(exact - pieces[0]))
    pieces.append(exact - pieces[0] - pieces[1])
    start = np.zeros((n_sp, 8, 2 * HEAD), np.float32)
    start[:, 0], start[:, 1] = pair(np.arange(n_sp) * rows)
    start[:, 2, :half], start[:, 2, half:HEAD] = -1.0, 1.0
    for row, value in zip(range(3, 7), (*pieces, exact)):
        start[:, row, :HEAD] = np.concatenate([value, value])
    return start, np.stack(pair(np.arange(rows)))


def kernel(
    rows,
    tokens,
    gain,
    w_query,
    w_key,
    w_value,
    w_pool,
    scale,
    sink,
    w_out,
    start_angles,
    row_angles,
    out,
    tok,
    nrm,
    gain_v,
    wk_v,
    wv_v,
    scale_v,
    sink_v,
    start_v,
    angles_v,
    wqp,
    kvbuf,
    wkv,
    wbuf,
    q_v,
    p_ext,
    pool_v,
    kv_ext,
    mix_send,
    mix_recv,
    load_sem,
    tok_sem,
    sent,
    got,
    x_sem,
    ring_sem,
):
    s = lax.axis_index("sp")
    t = lax.axis_index("tp")
    n_sp = lax.axis_size("sp")
    n_tp = lax.axis_size("tp")
    x, c = t // 2, t % 2
    z, y = s // RING, s % RING
    a = y + c * (z - y)
    b = z + c * (y - z)
    features = tok.shape[1]
    blocks = rows // QB
    half_blocks = blocks // 2

    def load(src, dst, i):
        return pltpu.make_async_copy(src, dst, load_sem.at[i])

    early = [
        load(w_key, wk_v, 0), load(w_value, wv_v, 1), load(w_out, wbuf.at[c, b, x, a], 2),
    ]
    late = [
        load(gain, gain_v, 3),
        load(w_query, wqp.at[pl.ds(0, HEAD)], 4), load(w_pool, wqp.at[pl.ds(HEAD, HEAD)], 5),
        load(row_angles, angles_v, 6), load(start_angles.at[s], start_v, 7),
        load(scale, scale_v, 8), load(sink, sink_v, 9),
    ]
    tok_loads = [
        pltpu.make_async_copy(
            tokens.at[pl.ds(i * QB, QB)], tok.at[pl.ds(i * QB, QB)], tok_sem.at[i]
        )
        for i in range(blocks)
    ]
    for copy in early:
        copy.start()

    step_a = 1 + (RING - 1) * c
    step_b = RING - (RING - 1) * c
    other = t + 1 - 2 * c

    def along_a(k):
        return (s + ((a + k) % RING - a) * step_a, t)

    def along_b(k):
        return (s + ((b + k) % RING - b) * step_b, t)

    def along_x(k):
        return (s, ((x + k) % 4) * 2 + c)

    def along_tp(k):
        return (s, (t + k) % n_tp)

    after = ((s + 1) % n_sp, t)
    before = ((s + n_sp - 1) % n_sp, t)

    barrier = pltpu.get_barrier_semaphore()
    peers = (
        [along_a(k) for k in ORDER]
        + [along_b(k) for k in ORDER]
        + [along_tp(k) for k in range(1, n_tp)]
        + [after, before]
    )
    for peer in peers:
        pl.semaphore_signal(barrier, inc=1, device_id=peer, device_id_type=MESH)
    for copy in (*tok_loads, *late):
        copy.start()

    def remote(src, dst, ssem, rsem, device):
        return pltpu.make_async_remote_copy(
            src_ref=src, dst_ref=dst, send_sem=ssem, recv_sem=rsem,
            device_id=device, device_id_type=MESH,
        )

    def landed(region, sem):
        remote(region, region, sem, sem, (s, other)).wait_recv()

    def left_here(region, sem):
        remote(region, region, sem, sem, (s, other)).wait_send()

    KV1, KV2, KVD, W1, W2, WD, PH, KH, MX, RR, RL = range(11)

    with jax.named_scope("load_wait"):
        for copy in early:
            copy.wait()

    lane = lax.broadcasted_iota(jnp.int32, (1, 2 * HEAD), 1)

    def swap_halves(value):
        return pltpu.roll(value, HEAD, 1)

    wk_f, wv_f = wk_v[...].astype(F32), wv_v[...].astype(F32)
    low_head = t < n_tp // 2
    k_part = jnp.where(low_head, wk_f, swap_halves(wk_f))
    v_part = jnp.where(low_head, swap_halves(wv_f), wv_f)
    kv_piece = jnp.where(lane < HEAD, k_part, v_part)
    half_rows = kv_piece.shape[0] // 2
    kvbuf[c, b, a] = jnp.where(c == 0, kv_piece[:half_rows], kv_piece[half_rows:]).astype(BF16)
    width = wbuf.shape[4]

    with jax.named_scope("barrier_wait"):
        pl.semaphore_wait(barrier, len(peers))

    own_kv, own_w = kvbuf.at[c, b, a], wbuf.at[c, b, x, a]
    for k in FAR_FIRST:
        remote(own_kv, own_kv, sent.at[KV1], got.at[KV1], along_a(k)).start()
    for k in FAR_FIRST:
        remote(own_w, own_w, sent.at[W1], got.at[W1], along_a(k)).start()

    chunk, slab = 32, 128

    def slabs():
        return [slice(j * slab, (j + 1) * slab) for j in range(features // slab)]

    def norm_at(i):
        return pl.ds(pl.multiple_of(i * chunk, chunk), chunk)

    def norm_center(i):
        parts = [tok[norm_at(i), cols].astype(F32) for cols in slabs()]
        while len(parts) > 1:
            parts = [p + q for p, q in zip(parts[::2], parts[1::2])]
        return jnp.sum(parts[0], axis=-1, keepdims=True) * (1.0 / features)

    def norm_spread(i, center):
        total = [0.0, 0.0]
        for j, cols in enumerate(slabs()):
            shifted = tok[norm_at(i), cols].astype(F32) - center
            total[j % 2] = total[j % 2] + shifted * shifted
        spread = jnp.sum(total[0] + total[1], axis=-1, keepdims=True) * (1.0 / features)
        return lax.rsqrt(spread + 1e-06)

    def norm_store(i, center, inverse):
        for cols in slabs():
            shifted = tok[norm_at(i), cols].astype(F32) - center
            nrm[norm_at(i), cols] = (shifted * inverse * gain_v[:, cols]).astype(BF16)

    def norm_blocks(lo, hi):
        for i in range(lo, hi):
            tok_loads[i].wait()
        lo, hi = lo * QB // chunk, hi * QB // chunk

        def step(i, carry):
            later, center, inverse = carry
            norm_store(i, center, inverse)
            next_inverse = norm_spread(jnp.minimum(i + 1, hi - 1), later)
            return norm_center(jnp.minimum(i + 2, hi - 1)), later, next_inverse

        first = norm_center(lo)
        lax.fori_loop(lo, hi, step, (norm_center(lo + 1), first, norm_spread(lo, first)))

    late[0].wait()
    with jax.named_scope("norm_a"):
        norm_blocks(0, half_blocks)
    with jax.named_scope("norm_b"):
        norm_blocks(half_blocks, half_blocks + 2)
    with jax.named_scope("kv1_wait"):
        landed(kvbuf.at[c, b, pl.ds(0, RING - 1)], got.at[KV1])
    line_kv = kvbuf.at[c, b]
    for k in FAR_FIRST:
        remote(line_kv, line_kv, sent.at[KV2], got.at[KV2], along_b(k)).start()
    with jax.named_scope("w1_wait"):
        landed(wbuf.at[c, b, x, pl.ds(0, RING - 1)], got.at[W1])

    def chunk_at(way, d):
        return (b + (RING - d if way == 0 else d)) % RING

    def part_at(owner, place, r):
        return wbuf.at[owner, place, (x + r) % 4]

    def ring_send(way, d, r):
        part = part_at(c, chunk_at(way, d), r)
        device = along_b(1 if way == 0 else RING - 1)
        remote(part, part, sent.at[RR + way], ring_sem.at[way, 4 * d + r], device).start()

    def cross(place, r):
        part = part_at(c, place, r)
        remote(part, part, sent.at[WD], got.at[WD], (s, other)).start()

    def ring_start(r):
        ring_send(0, 0, r)
        ring_send(1, 0, r)
        cross(b, r)

    def ring_advance(d, parts):
        with jax.named_scope("ring_wait"):
            for r in parts:
                for way in range(2):
                    if d == 4 and r // 2 != way:
                        continue
                    place = chunk_at(way, d)
                    landed(part_at(c, place, r), ring_sem.at[way, 4 * (d - 1) + r])
                    if d < 3 or (d == 3 and r // 2 == way):
                        ring_send(way, d, r)
                    cross(place, r)

    line_w = part_at(c, b, 0)
    for k in (2, 1, 3):
        remote(line_w, line_w, sent.at[W2], x_sem.at[k], along_x(k)).start()
    ring_start(0)

    with jax.named_scope("norm_c"):
        norm_blocks(half_blocks + 2, blocks)
    for copy in late[1:]:
        copy.wait()

    seq_total = n_sp * rows
    base_c, base_s = start_v[0:1, :], start_v[1:2, :]
    signed, piece_1, piece_2, piece_3, whole = (start_v[i : i + 1, :] for i in range(2, 7))
    turn_rows = 64

    def turn_block(i, carry):
        at = pl.ds(pl.multiple_of(i * turn_rows, turn_rows), turn_rows)
        row_c, row_s = angles_v[0, at, :], angles_v[1, at, :]
        cosine = base_c * row_c - base_s * row_s
        sine = base_s * row_c + base_c * row_s
        position = (
            lax.broadcasted_iota(jnp.int32, (turn_rows, 1), 0) + (s * rows + i * turn_rows)
        ).astype(F32)
        rounding = position * whole - position * piece_1
        rounding = rounding - position * piece_2 - position * piece_3
        rounding = rounding * signed
        angles_v[0, at, :] = cosine - rounding * sine
        angles_v[1, at, :] = sine + rounding * cosine
        return carry

    with jax.named_scope("turns"):
        lax.fori_loop(0, rows // turn_rows, turn_block, 0)

    def rotated(value, at):
        partner = jnp.where(
            lane < HEAD // 2,
            pltpu.roll(value, 2 * HEAD - HEAD // 2, 1),
            pltpu.roll(value, HEAD // 2, 1),
        )
        return value * angles_v[0, at, :] + partner * angles_v[1, at, :]

    wide = 2 * QB
    query_scale = jnp.where(lane < HEAD, HEAD ** (-0.5), 0.0)

    def query_block(i, carry):
        at = pl.ds(pl.multiple_of(i * wide, wide), wide)
        value = lax.dot_general(
            nrm[at, :], wqp[...], (((1,), (1,)), ((), ())), preferred_element_type=F32
        )
        p_ext[pl.ds(pl.multiple_of(EDGE + i * wide, EDGE), wide), :] = value.astype(BF16)
        q_v[at, :] = (rotated(value, at) * query_scale).astype(BF16)
        return carry

    with jax.named_scope("query_proj"):
        lax.fori_loop(0, rows // wide, query_block, 0)

    for source, target, device in ((rows, 0, after), (EDGE, EDGE + rows, before)):
        remote(
            p_ext.at[pl.ds(source, EDGE)], p_ext.at[pl.ds(target, EDGE)],
            sent.at[PH], got.at[PH], device,
        ).start()

    ring_advance(1, (0,))
    with jax.named_scope("w2_wait"):
        for k in (1, 3, 2):
            landed(part_at(c, b, 4 - k), x_sem.at[k])
            ring_start(4 - k)

    with jax.named_scope("kv2_wait"):
        landed(kvbuf.at[c, pl.ds(0, RING - 1)], got.at[KV2])
    remote(kvbuf.at[c], kvbuf.at[c], sent.at[KVD], got.at[KVD], (s, other)).start()

    with jax.named_scope("pool_halo"):
        landed(p_ext.at[pl.ds(0, 2 * EDGE)], got.at[PH])

    @pl.when(s == 0)
    def _():
        p_ext[pl.ds(0, EDGE), :] = jnp.zeros((EDGE, 2 * HEAD), BF16)

    @pl.when(s == n_sp - 1)
    def _():
        p_ext[pl.ds(EDGE + rows, EDGE), :] = jnp.zeros((EDGE, 2 * HEAD), BF16)

    reach = 1 + (t // 2 > 0) + 2 * (t // 2 > 1) + 4 * (t // 2 > 2)
    span = QB + 2 * EDGE
    apart = (
        lax.broadcasted_iota(jnp.int32, (QB, span), 1)
        - lax.broadcasted_iota(jnp.int32, (QB, span), 0) - EDGE
    )
    band = jnp.where((apart >= -reach) & (apart < reach), 1.0, 0.0).astype(BF16)
    row_id = lax.broadcasted_iota(jnp.int32, (QB, 1), 0)
    scales = jnp.concatenate([scale_v[...], scale_v[...]], axis=1)
    sinks = sink_v[...]

    def pool_block(i, carry):
        first = pl.multiple_of(i * QB, QB)
        sums = jnp.dot(band, p_ext[pl.ds(first, span), :], preferred_element_type=F32)
        position = row_id + (s * rows + first)
        counted = (
            jnp.minimum(position + reach, seq_total) - jnp.maximum(position - reach, 0)
        ).astype(F32)
        here = p_ext[pl.ds(pl.multiple_of(EDGE + first, EDGE), QB), :].astype(F32)
        pooled = (sums * (1.0 / counted) - here) * scales
        pool_v[pl.ds(first, QB), :] = swap_halves(pooled).astype(BF16)
        return carry

    with jax.named_scope("pool_mix"):
        lax.fori_loop(0, blocks, pool_block, 0, unroll=2)

    with jax.named_scope("kvd_wait"):
        landed(kvbuf.at[c], got.at[KVD])

    def join_rows(i, carry):
        for j in range(RING):
            at = pl.multiple_of((i * RING + j) * 2 * half_rows, 2 * half_rows)
            wkv[pl.ds(at, half_rows), :] = kvbuf[0, i, j]
            wkv[pl.ds(pl.multiple_of(at + half_rows, half_rows), half_rows), :] = kvbuf[1, j, i]
        return carry

    with jax.named_scope("kv_join"):
        lax.fori_loop(0, RING, join_rows, 0)

    def key_rows(first, count):
        at = pl.ds(pl.multiple_of(first, QB), count)
        value = jnp.dot(nrm[at, :], wkv[...], preferred_element_type=F32)
        kv_ext[pl.ds(pl.multiple_of(WINDOW + first, QB), count), :] = rotated(value, at).astype(BF16)

    with jax.named_scope("key_edge"):
        key_rows(0, QB)
        key_rows(rows - QB, QB)
    ring_advance(2, (0,))
    for source, target, device in ((rows, 0, after), (WINDOW, WINDOW + rows, before)):
        remote(
            kv_ext.at[pl.ds(source, WINDOW)], kv_ext.at[pl.ds(target, WINDOW)],
            sent.at[KH], got.at[KH], device,
        ).start()
    with jax.named_scope("key_rest"):
        key_rows(QB, wide)
        key_rows(QB + wide, wide)
    ring_advance(1, (1, 3, 2))
    with jax.named_scope("key_rest"):
        key_rows(QB + 2 * wide, wide)

    query_at = lax.broadcasted_iota(jnp.int32, (QB, QB), 0)
    key_at = lax.broadcasted_iota(jnp.int32, (QB, QB), 1)

    def attend(i):
        first = i * QB
        keys = kv_ext[pl.ds(first, QB + 2 * WINDOW), :]
        scores = lax.dot_general(
            q_v[pl.ds(first, QB), :], keys, (((1,), (1,)), ((), ())), preferred_element_type=F32
        )
        low_ok, high_ok = key_at >= query_at, key_at <= query_at
        if i == 0:
            low_ok = low_ok & (s > 0)
        if i == blocks - 1:
            high_ok = high_ok & (s < n_sp - 1)
        scores = jnp.concatenate(
            [
                jnp.where(low_ok, scores[:, :QB], NEG_BIG),
                scores[:, QB : 2 * QB],
                jnp.where(high_ok, scores[:, 2 * QB :], NEG_BIG),
            ],
            axis=1,
        )
        highest = jnp.maximum(jnp.max(scores, axis=-1, keepdims=True), sinks)
        expo = jnp.exp(scores - highest)
        total = jnp.sum(expo, axis=-1, keepdims=True) + jnp.exp(sinks - highest)
        weights = (expo * (1.0 / total)).astype(BF16)
        result = jnp.dot(weights, keys, preferred_element_type=F32)
        mix_send[i] = jnp.where(lane < HEAD, pool_v[pl.ds(first, QB), :].astype(F32), result).astype(BF16)

    def hand_over(i):
        @pl.when(i != t)
        def _():
            remote(mix_send.at[i], mix_recv.at[t], sent.at[MX], got.at[MX], (s, i)).start()

        @pl.when(i == t)
        def _():
            mix_recv[i] = mix_send[i]

    def attend_pair(i, j):
        with jax.named_scope("attend"):
            attend(i)
            attend(j)
        hand_over(i)
        hand_over(j)

    attend_pair(1, 2)
    ring_advance(3, (0,))
    attend_pair(3, 4)
    ring_advance(2, (1, 3, 2))
    attend_pair(5, 6)
    ring_advance(4, (0,))
    with jax.named_scope("key_halo"):
        landed(kv_ext.at[pl.ds(0, 2 * WINDOW)], got.at[KH])
    attend_pair(0, blocks - 1)
    ring_advance(3, (1, 3, 2))
    ring_advance(4, (1, 3, 2))

    with jax.named_scope("mix_wait"):
        landed(mix_recv.at[pl.ds(0, n_tp - 1)], got.at[MX])
    left, right = [], []
    for j in range(n_tp // 2):
        even, odd = mix_recv[2 * j].astype(F32), mix_recv[2 * j + 1].astype(F32)
        left.append(jnp.where(lane < HEAD, swap_halves(even), odd).astype(BF16))
        right.append(jnp.where(lane < HEAD, even, swap_halves(odd)).astype(BF16))
    mixed = jnp.concatenate(left + right, axis=1)

    with jax.named_scope("wd_wait"):
        landed(wbuf.at[c], got.at[WD])

    span_out = RING * width
    with jax.named_scope("out_proj"):
        for i in range(RING):
            parts = []
            for j in range(n_tp // 2):
                parts.append(wbuf[0, i, j].reshape(span_out, QB))
                parts.append(wbuf[1, :, j, i].reshape(span_out, QB))
            out[:, i * span_out : (i + 1) * span_out] = lax.dot_general(
                mixed, jnp.concatenate(parts, axis=1), (((1,), (1,)), ((), ())),
                preferred_element_type=F32,
            ).astype(BF16)

    with jax.named_scope("send_wait"):
        left_here(kvbuf.at[c, b, pl.ds(0, RING - 1)], sent.at[KV1])
        left_here(kvbuf.at[c, pl.ds(0, RING - 1)], sent.at[KV2])
        left_here(kvbuf.at[c], sent.at[KVD])
        left_here(wbuf.at[c, b, x, pl.ds(0, RING - 1)], sent.at[W1])
        left_here(wbuf.at[c, b, pl.ds(0, 3)], sent.at[W2])
        left_here(wbuf.at[c], sent.at[WD])
        left_here(wbuf.at[c, pl.ds(0, RING - 1), pl.ds(0, 2)], sent.at[RR])
        left_here(wbuf.at[c, pl.ds(0, RING - 1), pl.ds(0, 2)], sent.at[RL])
        left_here(p_ext.at[pl.ds(0, 2 * EDGE)], sent.at[PH])
        left_here(kv_ext.at[pl.ds(0, 2 * WINDOW)], sent.at[KH])
        left_here(mix_send.at[pl.ds(0, n_tp - 1)], sent.at[MX])


def body(tokens, norm_gain, w_query, w_key, w_value, w_pool_in, sink_logit, pool_scale, w_out):
    rows, features = tokens.shape
    n_sp, n_tp = lax.axis_size("sp"), lax.axis_size("tp")
    start, row = angle_tables(n_sp, rows)
    dma, vmem = pltpu.SemaphoreType.DMA, pltpu.VMEM
    half = w_key.shape[0] // 2
    width = w_out.shape[1]
    pair = 2 * HEAD
    scratch = [
        vmem((rows, features), BF16),
        vmem((rows, features), BF16),
        vmem((1, features), F32),
        vmem(w_key.shape, BF16),
        vmem(w_value.shape, BF16),
        vmem((1, HEAD), F32),
        vmem((1, 1), F32),
        vmem((8, pair), F32),
        vmem((2, rows, pair), F32),
        vmem((pair, features), BF16),
        vmem((2, RING, RING, half, pair), BF16),
        vmem((features, pair), BF16),
        vmem((2, RING, n_tp // 2, RING, width, w_out.shape[0]), BF16),
        vmem((rows, pair), BF16),
        vmem((rows + 2 * EDGE, pair), BF16),
        vmem((rows, pair), BF16),
        vmem((rows + 2 * WINDOW, pair), BF16),
        vmem((n_tp, QB, pair), BF16),
        vmem((n_tp, QB, pair), BF16),
        dma((10,)),
        dma((rows // QB,)),
        dma((11,)),
        dma((9,)),
        dma((4,)),
        dma((2, 16)),
    ]
    return pl.pallas_call(
        functools.partial(kernel, rows),
        name="mixer",
        out_shape=jax.ShapeDtypeStruct((rows // n_tp, w_out.shape[1] * n_sp), BF16),
        in_specs=[pl.BlockSpec(memory_space=pl.ANY)] * 11,
        out_specs=pl.BlockSpec(memory_space=pltpu.VMEM),
        scratch_shapes=scratch,
        compiler_params=pltpu.CompilerParams(
            collective_id=0, has_side_effects=True, vmem_limit_bytes=60 * 2**20
        ),
    )(
        tokens, norm_gain[None, :], w_query.T, w_key, w_value, w_pool_in.T, pool_scale[None, :], sink_logit[None, :], w_out.T,
        jnp.asarray(start), jnp.asarray(row),
    )


def solution(mesh):
    in_specs = (
        P("sp", None),
        P(),
        P(None, "tp"),
        P("sp", None),
        P("sp", None),
        P(None, "tp"),
        P("tp"),
        P("tp"),
        P("tp", "sp"),
    )
    out_specs = P(("sp", "tp"), None)
    return jax.shard_map(body, mesh=mesh, in_specs=in_specs, out_specs=out_specs, check_vma=False)
```

time: 55.1 us -> 49.7 us (0.902)
  Pallas kernels: 52.4 us -> 47 us
    pallas_call x1, Pallas kernels: 52.4 us -> 47 us  [body(): pl.pallas_call(functools.partial(kernel, rows), name='mixer', out_shape=j...]
where the time goes in v3:
time: 49.7 us; the launch traced here: 49.6 us
  Pallas kernels  47 us (95%)
  local copies, waits for them, and re-layouts  1.88 us (4%)
  between operations  0.66 us (1%)
    pallas_call x1, Pallas kernels, body(): pl.pallas_call(functools.partial(kernel, rows), name='mixer', out_shape=j...  47 us
    unnamed x1, local copies, waits for them, and re-layouts  1.88 us

profile of v3, /device:TPU:1, one launch (start us, length us, event | category | flops | bytes accessed | tf_op | source)
XLA Modules:
  0.0 49.6 jit_solution(17809973089736328194)
XLA Ops:
  0.7 47.0 %mixer.1 = bf16[128,2048]{1,0:T(8,128)(2,1)} custom-call(bf16[1024,2048]{1,0:T(8,128)(2,1)} %tokens.1, f32[1,2048]{1,0:T(1,128)} %bitcast.9, bf16[64,2048]{1,0:T(8,128)(2,1)} %bitcast.7, bf16[32,128]{1,0:T(8,128)(2,1)} %w_key.1, bf16[32,128]{1,0:T(8,128)(2,1)} %w_value.1, bf16[64,2048]{1,0:T(8,128)(2,1)} %bitcast.8, f32[1,64]{1,0:T(1,128)} %bitcast.11, ...), custom_call_target="tpu_custom_call" | custom-call | tf_op jit(solution)/shard_map/mixer/pallas_call | solution.py:556
  47.7 1.9 %copy.14 = bf16[128,2048]{1,0:T(8,128)(2,1)} copy(bf16[128,2048]{1,0:T(8,128)(2,1)} %mixer.1) | data formatting | bytes 1048576

commit v4 on v3

--- a/solution.py
+++ b/solution.py
@@ -82,12 +82,14 @@
     kv_ext,
     mix_send,
     mix_recv,
+    out_v,
     load_sem,
     tok_sem,
     sent,
     got,
     x_sem,
     ring_sem,
+    out_sem,
 ):
     s = lax.axis_index("sp")
     t = lax.axis_index("tp")
@@ -119,9 +121,6 @@
         )
         for i in range(blocks)
     ]
-    for copy in early:
-        copy.start()
-
     step_a = 1 + (RING - 1) * c
     step_b = RING - (RING - 1) * c
     other = t + 1 - 2 * c
@@ -142,16 +141,17 @@
     before = ((s + n_sp - 1) % n_sp, t)
 
     barrier = pltpu.get_barrier_semaphore()
-    peers = (
-        [along_a(k) for k in ORDER]
-        + [along_b(k) for k in ORDER]
-        + [along_tp(k) for k in range(1, n_tp)]
-        + [after, before]
-    )
-    for peer in peers:
-        pl.semaphore_signal(barrier, inc=1, device_id=peer, device_id_type=MESH)
-    for copy in (*tok_loads, *late):
+    far_peers = [along_a(k) for k in FAR_FIRST] + [along_b(k) for k in FAR_FIRST]
+    near_peers = [along_tp(k) for k in range(1, n_tp)] + [after, before]
+
+    def greet(devices):
+        for peer in devices:
+            pl.semaphore_signal(barrier, inc=1, device_id=peer, device_id_type=MESH)
+
+    greet(far_peers)
+    for copy in early:
         copy.start()
+    greet(near_peers)
 
     def remote(src, dst, ssem, rsem, device):
         return pltpu.make_async_remote_copy(
@@ -165,7 +165,7 @@
     def left_here(region, sem):
         remote(region, region, sem, sem, (s, other)).wait_send()
 
-    KV1, KV2, KVD, W1, W2, WD, PH, KH, MX, RR, RL = range(11)
+    KV1, KV2, KVD, W1, W2, WD, PH, KH, MX, D4, X4, RR, RL, WL = range(14)
 
     with jax.named_scope("load_wait"):
         for copy in early:
@@ -185,8 +185,11 @@
     kvbuf[c, b, a] = jnp.where(c == 0, kv_piece[:half_rows], kv_piece[half_rows:]).astype(BF16)
     width = wbuf.shape[4]
 
+    for copy in (late[0], *tok_loads, *late[1:]):
+        copy.start()
+
     with jax.named_scope("barrier_wait"):
-        pl.semaphore_wait(barrier, len(peers))
+        pl.semaphore_wait(barrier, len(far_peers) + len(near_peers))
 
     own_kv, own_w = kvbuf.at[c, b, a], wbuf.at[c, b, x, a]
     for k in FAR_FIRST:
@@ -240,6 +243,28 @@
         norm_blocks(0, half_blocks)
     with jax.named_scope("norm_b"):
         norm_blocks(half_blocks, half_blocks + 2)
+    with jax.named_scope("norm_c"):
+        norm_blocks(half_blocks + 2, blocks)
+    def rotated(value, at):
+        partner = jnp.where(
+            lane < HEAD // 2,
+            pltpu.roll(value, 2 * HEAD - HEAD // 2, 1),
+            pltpu.roll(value, HEAD // 2, 1),
+        )
+        return value * angles_v[0, at, :] + partner * angles_v[1, at, :]
+
+    wide = 2 * QB
+    query_scale = jnp.where(lane < HEAD, HEAD ** (-0.5), 0.0)
+
+    def query_block(i, carry):
+        at = pl.ds(pl.multiple_of(i * wide, wide), wide)
+        value = lax.dot_general(
+            nrm[at, :], wqp[...], (((1,), (1,)), ((), ())), preferred_element_type=F32
+        )
+        p_ext[pl.ds(pl.multiple_of(EDGE + i * wide, EDGE), wide), :] = value.astype(BF16)
+        q_v[at, :] = (rotated(value, at) * query_scale).astype(BF16)
+        return carry
+
     with jax.named_scope("kv1_wait"):
         landed(kvbuf.at[c, b, pl.ds(0, RING - 1)], got.at[KV1])
     line_kv = kvbuf.at[c, b]
@@ -259,9 +284,9 @@
         device = along_b(1 if way == 0 else RING - 1)
         remote(part, part, sent.at[RR + way], ring_sem.at[way, 4 * d + r], device).start()
 
-    def cross(place, r):
+    def cross(place, r, group=WD):
         part = part_at(c, place, r)
-        remote(part, part, sent.at[WD], got.at[WD], (s, other)).start()
+        remote(part, part, sent.at[group], got.at[group], (s, other)).start()
 
     def ring_start(r):
         ring_send(0, 0, r)
@@ -272,21 +297,33 @@
         with jax.named_scope("ring_wait"):
             for r in parts:
                 for way in range(2):
-                    if d == 4 and r // 2 != way:
-                        continue
                     place = chunk_at(way, d)
                     landed(part_at(c, place, r), ring_sem.at[way, 4 * (d - 1) + r])
-                    if d < 3 or (d == 3 and r // 2 == way):
+                    if d < 3:
                         ring_send(way, d, r)
-                    cross(place, r)
+                    cross(place, r, WL if d == 3 else WD)
 
     line_w = part_at(c, b, 0)
     for k in (2, 1, 3):
         remote(line_w, line_w, sent.at[W2], x_sem.at[k], along_x(k)).start()
     ring_start(0)
-
-    with jax.named_scope("norm_c"):
-        norm_blocks(half_blocks + 2, blocks)
+    remote(line_w, line_w, sent.at[D4], got.at[D4], along_b(4)).start()
+    far = (b + 4) % RING
+
+    def far_advance():
+        with jax.named_scope("far_wait"):
+            landed(part_at(c, far, 0), got.at[D4])
+        for k in (2, 1, 3):
+            part = part_at(c, far, 0)
+            remote(part, part, sent.at[X4], got.at[X4], along_x(k)).start()
+        cross(far, 0)
+
+    def far_finish():
+        with jax.named_scope("far_wait"):
+            landed(wbuf.at[c, far, pl.ds(0, 3)], got.at[X4])
+        for r in (1, 2, 3):
+            cross(far, r)
+
     for copy in late[1:]:
         copy.wait()
 
@@ -313,36 +350,17 @@
     with jax.named_scope("turns"):
         lax.fori_loop(0, rows // turn_rows, turn_block, 0)
 
-    def rotated(value, at):
-        partner = jnp.where(
-            lane < HEAD // 2,
-            pltpu.roll(value, 2 * HEAD - HEAD // 2, 1),
-            pltpu.roll(value, HEAD // 2, 1),
-        )
-        return value * angles_v[0, at, :] + partner * angles_v[1, at, :]
-
-    wide = 2 * QB
-    query_scale = jnp.where(lane < HEAD, HEAD ** (-0.5), 0.0)
-
-    def query_block(i, carry):
-        at = pl.ds(pl.multiple_of(i * wide, wide), wide)
-        value = lax.dot_general(
-            nrm[at, :], wqp[...], (((1,), (1,)), ((), ())), preferred_element_type=F32
-        )
-        p_ext[pl.ds(pl.multiple_of(EDGE + i * wide, EDGE), wide), :] = value.astype(BF16)
-        q_v[at, :] = (rotated(value, at) * query_scale).astype(BF16)
-        return carry
-
-    with jax.named_scope("query_proj"):
-        lax.fori_loop(0, rows // wide, query_block, 0)
-
+    with jax.named_scope("query_edge"):
+        query_block(0, 0)
+        query_block(rows // wide - 1, 0)
     for source, target, device in ((rows, 0, after), (EDGE, EDGE + rows, before)):
         remote(
             p_ext.at[pl.ds(source, EDGE)], p_ext.at[pl.ds(target, EDGE)],
             sent.at[PH], got.at[PH], device,
         ).start()
-
-    ring_advance(1, (0,))
+    with jax.named_scope("query_rest"):
+        lax.fori_loop(1, rows // wide - 1, query_block, 0)
+
     with jax.named_scope("w2_wait"):
         for k in (1, 3, 2):
             landed(part_at(c, b, 4 - k), x_sem.at[k])
@@ -352,6 +370,7 @@
         landed(kvbuf.at[c, pl.ds(0, RING - 1)], got.at[KV2])
     remote(kvbuf.at[c], kvbuf.at[c], sent.at[KVD], got.at[KVD], (s, other)).start()
 
+    ring_advance(1, (0,))
     with jax.named_scope("pool_halo"):
         landed(p_ext.at[pl.ds(0, 2 * EDGE)], got.at[PH])
 
@@ -372,7 +391,7 @@
     band = jnp.where((apart >= -reach) & (apart < reach), 1.0, 0.0).astype(BF16)
     row_id = lax.broadcasted_iota(jnp.int32, (QB, 1), 0)
     scales = jnp.concatenate([scale_v[...], scale_v[...]], axis=1)
-    sinks = sink_v[...]
+    sinks = jnp.broadcast_to(sink_v[...], (1, 2 * HEAD))
 
     def pool_block(i, carry):
         first = pl.multiple_of(i * QB, QB)
@@ -410,47 +429,64 @@
     with jax.named_scope("key_edge"):
         key_rows(0, QB)
         key_rows(rows - QB, QB)
-    ring_advance(2, (0,))
+    with jax.named_scope("key_rest"):
+        key_rows(QB, wide)
     for source, target, device in ((rows, 0, after), (WINDOW, WINDOW + rows, before)):
         remote(
             kv_ext.at[pl.ds(source, WINDOW)], kv_ext.at[pl.ds(target, WINDOW)],
             sent.at[KH], got.at[KH], device,
         ).start()
     with jax.named_scope("key_rest"):
-        key_rows(QB, wide)
         key_rows(QB + wide, wide)
-    ring_advance(1, (1, 3, 2))
-    with jax.named_scope("key_rest"):
         key_rows(QB + 2 * wide, wide)
 
     query_at = lax.broadcasted_iota(jnp.int32, (QB, QB), 0)
     key_at = lax.broadcasted_iota(jnp.int32, (QB, QB), 1)
 
-    def attend(i):
-        first = i * QB
-        keys = kv_ext[pl.ds(first, QB + 2 * WINDOW), :]
-        scores = lax.dot_general(
-            q_v[pl.ds(first, QB), :], keys, (((1,), (1,)), ((), ())), preferred_element_type=F32
-        )
-        low_ok, high_ok = key_at >= query_at, key_at <= query_at
-        if i == 0:
-            low_ok = low_ok & (s > 0)
-        if i == blocks - 1:
-            high_ok = high_ok & (s < n_sp - 1)
-        scores = jnp.concatenate(
-            [
-                jnp.where(low_ok, scores[:, :QB], NEG_BIG),
-                scores[:, QB : 2 * QB],
-                jnp.where(high_ok, scores[:, 2 * QB :], NEG_BIG),
-            ],
-            axis=1,
-        )
-        highest = jnp.maximum(jnp.max(scores, axis=-1, keepdims=True), sinks)
-        expo = jnp.exp(scores - highest)
-        total = jnp.sum(expo, axis=-1, keepdims=True) + jnp.exp(sinks - highest)
-        weights = (expo * (1.0 / total)).astype(BF16)
-        result = jnp.dot(weights, keys, preferred_element_type=F32)
-        mix_send[i] = jnp.where(lane < HEAD, pool_v[pl.ds(first, QB), :].astype(F32), result).astype(BF16)
+    def across_lanes(column):
+        return jnp.broadcast_to(column, (QB, 2 * HEAD))
+
+    def attend(blocks_now):
+        window = [kv_ext[pl.ds(i * QB, QB + 2 * WINDOW), :] for i in blocks_now]
+        scores = [
+            lax.dot_general(
+                q_v[pl.ds(i * QB, QB), :], keys, (((1,), (1,)), ((), ())),
+                preferred_element_type=F32,
+            )
+            for i, keys in zip(blocks_now, window)
+        ]
+        tiles = []
+        for i, score in zip(blocks_now, scores):
+            low_ok, high_ok = key_at >= query_at, key_at <= query_at
+            if i == 0:
+                low_ok = low_ok & (s > 0)
+            if i == blocks - 1:
+                high_ok = high_ok & (s < n_sp - 1)
+            tiles.append((
+                jnp.where(low_ok, score[:, :QB], NEG_BIG),
+                score[:, QB : 2 * QB],
+                jnp.where(high_ok, score[:, 2 * QB :], NEG_BIG),
+            ))
+        highest = [
+            jnp.max(jnp.maximum(jnp.maximum(p, q), r), axis=-1, keepdims=True) for p, q, r in tiles
+        ]
+        highest = [jnp.maximum(across_lanes(top), sinks) for top in highest]
+        expo = [[jnp.exp(part - top) for part in three] for three, top in zip(tiles, highest)]
+        total = [jnp.sum(p + q + r, axis=-1, keepdims=True) for p, q, r in expo]
+        inverse = [
+            1.0 / (across_lanes(some) + jnp.exp(sinks - top)) for some, top in zip(total, highest)
+        ]
+        weights = [
+            jnp.concatenate([(part * one).astype(BF16) for part in three], axis=1)
+            for three, one in zip(expo, inverse)
+        ]
+        result = [
+            jnp.dot(some, keys, preferred_element_type=F32) for some, keys in zip(weights, window)
+        ]
+        for i, some in zip(blocks_now, result):
+            mix_send[i] = jnp.where(
+                lane < HEAD, pool_v[pl.ds(i * QB, QB), :].astype(F32), some
+            ).astype(BF16)
 
     def hand_over(i):
         @pl.when(i != t)
@@ -463,23 +499,42 @@
 
     def attend_pair(i, j):
         with jax.named_scope("attend"):
-            attend(i)
-            attend(j)
+            attend((i, j))
         hand_over(i)
         hand_over(j)
 
+    far_advance()
+    ring_advance(1, (3,))
     attend_pair(1, 2)
-    ring_advance(3, (0,))
+    ring_advance(1, (1,))
     attend_pair(3, 4)
-    ring_advance(2, (1, 3, 2))
+    ring_advance(1, (2,))
     attend_pair(5, 6)
-    ring_advance(4, (0,))
+    ring_advance(2, (0,))
     with jax.named_scope("key_halo"):
         landed(kv_ext.at[pl.ds(0, 2 * WINDOW)], got.at[KH])
     attend_pair(0, blocks - 1)
-    ring_advance(3, (1, 3, 2))
-    ring_advance(4, (1, 3, 2))
-
+    ring_advance(2, (3,))
+    ring_advance(2, (1,))
+    ring_advance(2, (2,))
+    far_finish()
+    ring_advance(3, (0,))
+
+    def group_region(owner, group):
+        return wbuf.at[owner, pl.ds(0, 2 if group == WL else RING - 2)]
+
+    def cross_wait(group):
+        with jax.named_scope("cross_wait"):
+            landed(group_region(1 - c, group), got.at[group])
+
+    ring_advance(3, (3, 1, 2))
+    cross_wait(WD)
+
+    @pl.when(c == 0)
+    def _():
+        cross_wait(WL)
+
+    left_here(kvbuf.at[c, b, pl.ds(0, RING - 1)], sent.at[KV1])
     with jax.named_scope("mix_wait"):
         landed(mix_recv.at[pl.ds(0, n_tp - 1)], got.at[MX])
     left, right = [], []
@@ -489,30 +544,49 @@
         right.append(jnp.where(lane < HEAD, even, swap_halves(odd)).astype(BF16))
     mixed = jnp.concatenate(left + right, axis=1)
 
-    with jax.named_scope("wd_wait"):
-        landed(wbuf.at[c], got.at[WD])
-
     span_out = RING * width
-    with jax.named_scope("out_proj"):
-        for i in range(RING):
-            parts = []
-            for j in range(n_tp // 2):
-                parts.append(wbuf[0, i, j].reshape(span_out, QB))
-                parts.append(wbuf[1, :, j, i].reshape(span_out, QB))
-            out[:, i * span_out : (i + 1) * span_out] = lax.dot_general(
-                mixed, jnp.concatenate(parts, axis=1), (((1,), (1,)), ((), ())),
-                preferred_element_type=F32,
-            ).astype(BF16)
+    stores = []
+
+    def out_block(d):
+        i = (z + d) % RING
+        parts = []
+        for j in range(n_tp // 2):
+            parts.append(wbuf[0, i, j].reshape(span_out, QB))
+            parts.append(wbuf[1, :, j, i].reshape(span_out, QB))
+        cols = pl.ds(pl.multiple_of(i * span_out, span_out), span_out)
+        out_v[:, cols] = lax.dot_general(
+            mixed, jnp.concatenate(parts, axis=1), (((1,), (1,)), ((), ())),
+            preferred_element_type=F32,
+        ).astype(BF16)
+        store = pltpu.make_async_copy(out_v.at[:, cols], out.at[:, cols], out_sem.at[d])
+        store.start()
+        stores.append(store)
+
+    with jax.named_scope("out_most"):
+        for d in (0, 1, 7, 2, 6, 4):
+            out_block(d)
+
+    @pl.when(c == 1)
+    def _():
+        cross_wait(WL)
+
+    with jax.named_scope("out_last"):
+        for d in (3, 5):
+            out_block(d)
 
     with jax.named_scope("send_wait"):
-        left_here(kvbuf.at[c, b, pl.ds(0, RING - 1)], sent.at[KV1])
+        for store in stores:
+            store.wait()
         left_here(kvbuf.at[c, pl.ds(0, RING - 1)], sent.at[KV2])
         left_here(kvbuf.at[c], sent.at[KVD])
         left_here(wbuf.at[c, b, x, pl.ds(0, RING - 1)], sent.at[W1])
         left_here(wbuf.at[c, b, pl.ds(0, 3)], sent.at[W2])
-        left_here(wbuf.at[c], sent.at[WD])
-        left_here(wbuf.at[c, pl.ds(0, RING - 1), pl.ds(0, 2)], sent.at[RR])
-        left_here(wbuf.at[c, pl.ds(0, RING - 1), pl.ds(0, 2)], sent.at[RL])
+        left_here(group_region(c, WD), sent.at[WD])
+        left_here(group_region(c, WL), sent.at[WL])
+        left_here(part_at(c, b, 0), sent.at[D4])
+        left_here(wbuf.at[c, far, pl.ds(0, 3)], sent.at[X4])
+        left_here(wbuf.at[c, pl.ds(0, 3)], sent.at[RR])
+        left_here(wbuf.at[c, pl.ds(0, 3)], sent.at[RL])
         left_here(p_ext.at[pl.ds(0, 2 * EDGE)], sent.at[PH])
         left_here(kv_ext.at[pl.ds(0, 2 * WINDOW)], sent.at[KH])
         left_here(mix_send.at[pl.ds(0, n_tp - 1)], sent.at[MX])
@@ -546,19 +620,21 @@
         vmem((rows + 2 * WINDOW, pair), BF16),
         vmem((n_tp, QB, pair), BF16),
         vmem((n_tp, QB, pair), BF16),
+        vmem((rows // n_tp, width * n_sp), BF16),
         dma((10,)),
         dma((rows // QB,)),
-        dma((11,)),
-        dma((9,)),
+        dma((14,)),
+        dma((14,)),
         dma((4,)),
-        dma((2, 16)),
+        dma((2, 12)),
+        dma((RING,)),
     ]
     return pl.pallas_call(
         functools.partial(kernel, rows),
         name="mixer",
         out_shape=jax.ShapeDtypeStruct((rows // n_tp, w_out.shape[1] * n_sp), BF16),
         in_specs=[pl.BlockSpec(memory_space=pl.ANY)] * 11,
-        out_specs=pl.BlockSpec(memory_space=pltpu.VMEM),
+        out_specs=pl.BlockSpec(memory_space=pl.ANY),
         scratch_shapes=scratch,
         compiler_params=pltpu.CompilerParams(
             collective_id=0, has_side_effects=True, vmem_limit_bytes=60 * 2**20

time: 49.7 us -> 44.3 us (0.89)
  Pallas kernels: 47 us -> 41.6 us
    pallas_call x1, Pallas kernels: 47 us -> 41.6 us  [body(): pl.pallas_call(functools.partial(kernel, rows), name='mixer', out_shape=j...]
where the time goes in v4:
time: 44.3 us; the launch traced here: 44.1 us
  Pallas kernels  41.6 us (94%)
  local copies, waits for them, and re-layouts  1.88 us (4%)
  between operations  0.66 us (1%)
    pallas_call x1, Pallas kernels, body(): pl.pallas_call(functools.partial(kernel, rows), name='mixer', out_shape=j...  41.6 us
    unnamed x1, local copies, waits for them, and re-layouts  1.88 us

profile of v4, /device:TPU:1, one launch (start us, length us, event | category | flops | bytes accessed | tf_op | source)
XLA Modules:
  0.0 44.1 jit_solution(16832697897511999974)
XLA Ops:
  0.7 41.6 %mixer.1 = bf16[128,2048]{1,0:T(8,128)(2,1)} custom-call(bf16[1024,2048]{1,0:T(8,128)(2,1)} %tokens.1, f32[1,2048]{1,0:T(1,128)} %bitcast.9, bf16[64,2048]{1,0:T(8,128)(2,1)} %bitcast.7, bf16[32,128]{1,0:T(8,128)(2,1)} %w_key.1, bf16[32,128]{1,0:T(8,128)(2,1)} %w_value.1, bf16[64,2048]{1,0:T(8,128)(2,1)} %bitcast.8, f32[1,64]{1,0:T(1,128)} %bitcast.11, ...), custom_call_target="tpu_custom_call" | custom-call | tf_op jit(solution)/shard_map/mixer/pallas_call | solution.py:632
  42.2 1.9 %copy.14 = bf16[128,2048]{1,0:T(8,128)(2,1)} copy(bf16[128,2048]{1,0:T(8,128)(2,1)} %mixer.1) | data formatting | bytes 1048576

commit v5 on v4

--- a/solution.py
+++ b/solution.py
@@ -143,6 +143,8 @@
     barrier = pltpu.get_barrier_semaphore()
     far_peers = [along_a(k) for k in FAR_FIRST] + [along_b(k) for k in FAR_FIRST]
     near_peers = [along_tp(k) for k in range(1, n_tp)] + [after, before]
+    for k in (1, RING - 1):
+        near_peers += [(along_a(k)[0], other), (along_b(k)[0], other)]
 
     def greet(devices):
         for peer in devices:
@@ -165,7 +167,7 @@
     def left_here(region, sem):
         remote(region, region, sem, sem, (s, other)).wait_send()
 
-    KV1, KV2, KVD, W1, W2, WD, PH, KH, MX, D4, X4, RR, RL, WL = range(14)
+    KV1, KV2, KVD, W1, W2, WD, PH, KH, MX, D4, X4, RR, RL, WR, WL = range(15)
 
     with jax.named_scope("load_wait"):
         for copy in early:
@@ -193,9 +195,9 @@
 
     own_kv, own_w = kvbuf.at[c, b, a], wbuf.at[c, b, x, a]
     for k in FAR_FIRST:
+        remote(own_w, own_w, sent.at[W1], got.at[W1], along_a(k)).start()
+    for k in FAR_FIRST:
         remote(own_kv, own_kv, sent.at[KV1], got.at[KV1], along_a(k)).start()
-    for k in FAR_FIRST:
-        remote(own_w, own_w, sent.at[W1], got.at[W1], along_a(k)).start()
 
     chunk, slab = 32, 128
 
@@ -265,47 +267,60 @@
         q_v[at, :] = (rotated(value, at) * query_scale).astype(BF16)
         return carry
 
+    with jax.named_scope("w1_wait"):
+        landed(wbuf.at[c, b, x, pl.ds(0, RING - 1)], got.at[W1])
+
+    def chunk_at(way, d):
+        return (b + (RING - d if way == 0 else d)) % RING
+
+    def part_at(owner, place, r):
+        return wbuf.at[owner, place, (x + r) % 4]
+
+    def ring_send(way, d, r):
+        part = part_at(c, chunk_at(way, d), r)
+        device = along_b(1 if way == 0 else RING - 1)
+        remote(part, part, sent.at[RR + way], ring_sem.at[way, 4 * d + r], device).start()
+
+    def cross(place, r, group=WD):
+        part = part_at(c, place, r)
+        remote(part, part, sent.at[group], got.at[group], (s, other)).start()
+
+    def ring_start(r):
+        ring_send(0, 0, r)
+        ring_send(1, 0, r)
+        cross(b, r)
+
+    def ring_event(d, r, way):
+        place = chunk_at(way, d)
+        part = part_at(c, place, r)
+        landed(part, ring_sem.at[way, 4 * (d - 1) + r])
+        last = (WR, WL)[way]
+        if d < 3:
+            ring_send(way, d, r)
+        if d == 2 and r == 2:
+            beside = (along_b(1 if way == 0 else RING - 1)[0], other)
+            remote(part, part, sent.at[last], got.at[last], beside).start()
+        if d < 3:
+            cross(place, r)
+        elif r != 2:
+            cross(place, r, last)
+
+    def ring_advance(d, parts):
+        events = [(r, way) for r in parts for way in range(2)]
+        if d == 3:
+            events = [(r, way) for way in (1, 0) for r in parts]
+        with jax.named_scope("ring_wait"):
+            for r, way in events:
+                ring_event(d, r, way)
+
+    line_w = part_at(c, b, 0)
+    for k in (2, 1, 3):
+        remote(line_w, line_w, sent.at[W2], x_sem.at[k], along_x(k)).start()
     with jax.named_scope("kv1_wait"):
         landed(kvbuf.at[c, b, pl.ds(0, RING - 1)], got.at[KV1])
     line_kv = kvbuf.at[c, b]
     for k in FAR_FIRST:
         remote(line_kv, line_kv, sent.at[KV2], got.at[KV2], along_b(k)).start()
-    with jax.named_scope("w1_wait"):
-        landed(wbuf.at[c, b, x, pl.ds(0, RING - 1)], got.at[W1])
-
-    def chunk_at(way, d):
-        return (b + (RING - d if way == 0 else d)) % RING
-
-    def part_at(owner, place, r):
-        return wbuf.at[owner, place, (x + r) % 4]
-
-    def ring_send(way, d, r):
-        part = part_at(c, chunk_at(way, d), r)
-        device = along_b(1 if way == 0 else RING - 1)
-        remote(part, part, sent.at[RR + way], ring_sem.at[way, 4 * d + r], device).start()
-
-    def cross(place, r, group=WD):
-        part = part_at(c, place, r)
-        remote(part, part, sent.at[group], got.at[group], (s, other)).start()
-
-    def ring_start(r):
-        ring_send(0, 0, r)
-        ring_send(1, 0, r)
-        cross(b, r)
-
-    def ring_advance(d, parts):
-        with jax.named_scope("ring_wait"):
-            for r in parts:
-                for way in range(2):
-                    place = chunk_at(way, d)
-                    landed(part_at(c, place, r), ring_sem.at[way, 4 * (d - 1) + r])
-                    if d < 3:
-                        ring_send(way, d, r)
-                    cross(place, r, WL if d == 3 else WD)
-
-    line_w = part_at(c, b, 0)
-    for k in (2, 1, 3):
-        remote(line_w, line_w, sent.at[W2], x_sem.at[k], along_x(k)).start()
     ring_start(0)
     remote(line_w, line_w, sent.at[D4], got.at[D4], along_b(4)).start()
     far = (b + 4) % RING
@@ -429,6 +444,7 @@
     with jax.named_scope("key_edge"):
         key_rows(0, QB)
         key_rows(rows - QB, QB)
+    ring_advance(1, (3,))
     with jax.named_scope("key_rest"):
         key_rows(QB, wide)
     for source, target, device in ((rows, 0, after), (WINDOW, WINDOW + rows, before)):
@@ -436,8 +452,12 @@
             kv_ext.at[pl.ds(source, WINDOW)], kv_ext.at[pl.ds(target, WINDOW)],
             sent.at[KH], got.at[KH], device,
         ).start()
+    far_advance()
+    ring_advance(1, (1,))
     with jax.named_scope("key_rest"):
         key_rows(QB + wide, wide)
+    ring_advance(1, (2,))
+    with jax.named_scope("key_rest"):
         key_rows(QB + 2 * wide, wide)
 
     query_at = lax.broadcasted_iota(jnp.int32, (QB, QB), 0)
@@ -503,36 +523,32 @@
         hand_over(i)
         hand_over(j)
 
-    far_advance()
-    ring_advance(1, (3,))
     attend_pair(1, 2)
-    ring_advance(1, (1,))
     attend_pair(3, 4)
-    ring_advance(1, (2,))
+    ring_advance(2, (0,))
     attend_pair(5, 6)
-    ring_advance(2, (0,))
+    ring_advance(2, (3,))
     with jax.named_scope("key_halo"):
         landed(kv_ext.at[pl.ds(0, 2 * WINDOW)], got.at[KH])
     attend_pair(0, blocks - 1)
-    ring_advance(2, (3,))
     ring_advance(2, (1,))
     ring_advance(2, (2,))
     far_finish()
-    ring_advance(3, (0,))
 
     def group_region(owner, group):
-        return wbuf.at[owner, pl.ds(0, 2 if group == WL else RING - 2)]
+        return wbuf.at[owner, pl.ds(0, RING - 2 if group == WD else 1)]
 
     def cross_wait(group):
         with jax.named_scope("cross_wait"):
             landed(group_region(1 - c, group), got.at[group])
 
-    ring_advance(3, (3, 1, 2))
+    ring_advance(3, (0, 3, 1, 2))
     cross_wait(WD)
 
     @pl.when(c == 0)
     def _():
         cross_wait(WL)
+        cross_wait(WR)
 
     left_here(kvbuf.at[c, b, pl.ds(0, RING - 1)], sent.at[KV1])
     with jax.named_scope("mix_wait"):
@@ -545,7 +561,6 @@
     mixed = jnp.concatenate(left + right, axis=1)
 
     span_out = RING * width
-    stores = []
 
     def out_block(d):
         i = (z + d) % RING
@@ -558,31 +573,30 @@
             mixed, jnp.concatenate(parts, axis=1), (((1,), (1,)), ((), ())),
             preferred_element_type=F32,
         ).astype(BF16)
-        store = pltpu.make_async_copy(out_v.at[:, cols], out.at[:, cols], out_sem.at[d])
+        store = pltpu.make_async_copy(out_v.at[:, cols], out.at[:, cols], out_sem.at[0])
         store.start()
-        stores.append(store)
 
     with jax.named_scope("out_most"):
         for d in (0, 1, 7, 2, 6, 4):
             out_block(d)
 
-    @pl.when(c == 1)
-    def _():
-        cross_wait(WL)
-
-    with jax.named_scope("out_last"):
-        for d in (3, 5):
+    for d, group in ((3, WL), (5, WR)):
+        @pl.when(c == 1)
+        def _():
+            cross_wait(group)
+
+        with jax.named_scope("out_last"):
             out_block(d)
 
     with jax.named_scope("send_wait"):
-        for store in stores:
-            store.wait()
+        pltpu.make_async_copy(out_v, out, out_sem.at[0]).wait()
         left_here(kvbuf.at[c, pl.ds(0, RING - 1)], sent.at[KV2])
         left_here(kvbuf.at[c], sent.at[KVD])
         left_here(wbuf.at[c, b, x, pl.ds(0, RING - 1)], sent.at[W1])
         left_here(wbuf.at[c, b, pl.ds(0, 3)], sent.at[W2])
         left_here(group_region(c, WD), sent.at[WD])
         left_here(group_region(c, WL), sent.at[WL])
+        left_here(group_region(c, WR), sent.at[WR])
         left_here(part_at(c, b, 0), sent.at[D4])
         left_here(wbuf.at[c, far, pl.ds(0, 3)], sent.at[X4])
         left_here(wbuf.at[c, pl.ds(0, 3)], sent.at[RR])
@@ -623,11 +637,11 @@
         vmem((rows // n_tp, width * n_sp), BF16),
         dma((10,)),
         dma((rows // QB,)),
-        dma((14,)),
-        dma((14,)),
+        dma((15,)),
+        dma((15,)),
         dma((4,)),
         dma((2, 12)),
-        dma((RING,)),
+        dma((1,)),
     ]
     return pl.pallas_call(
         functools.partial(kernel, rows),

time: 44.3 us -> 43.9 us (level)
  Pallas kernels: 41.6 us -> 41.1 us
    pallas_call x1, Pallas kernels: 41.6 us -> 41.1 us  [body(): pl.pallas_call(functools.partial(kernel, rows), name='mixer', out_shape=j...]
where the time goes in v5:
time: 43.9 us; the launch traced here: 43.7 us
  Pallas kernels  41.1 us (94%)
  local copies, waits for them, and re-layouts  1.88 us (4%)
  between operations  0.66 us (2%)
    pallas_call x1, Pallas kernels, body(): pl.pallas_call(functools.partial(kernel, rows), name='mixer', out_shape=j...  41.1 us
    unnamed x1, local copies, waits for them, and re-layouts  1.88 us

profile of v5, /device:TPU:1, one launch (start us, length us, event | category | flops | bytes accessed | tf_op | source)
XLA Modules:
  0.0 43.7 jit_solution(6563548584650443261)
XLA Ops:
  0.7 41.1 %mixer.1 = bf16[128,2048]{1,0:T(8,128)(2,1)} custom-call(bf16[1024,2048]{1,0:T(8,128)(2,1)} %tokens.1, f32[1,2048]{1,0:T(1,128)} %bitcast.9, bf16[64,2048]{1,0:T(8,128)(2,1)} %bitcast.7, bf16[32,128]{1,0:T(8,128)(2,1)} %w_key.1, bf16[32,128]{1,0:T(8,128)(2,1)} %w_value.1, bf16[64,2048]{1,0:T(8,128)(2,1)} %bitcast.8, f32[1,64]{1,0:T(1,128)} %bitcast.11, ...), custom_call_target="tpu_custom_call" | custom-call | tf_op jit(solution)/shard_map/mixer/pallas_call | solution.py:646
  41.8 1.9 %copy.14 = bf16[128,2048]{1,0:T(8,128)(2,1)} copy(bf16[128,2048]{1,0:T(8,128)(2,1)} %mixer.1) | data formatting | bytes 1048576

commit v6 on v5

--- a/solution.py
+++ b/solution.py
@@ -441,10 +441,11 @@
         value = jnp.dot(nrm[at, :], wkv[...], preferred_element_type=F32)
         kv_ext[pl.ds(pl.multiple_of(WINDOW + first, QB), count), :] = rotated(value, at).astype(BF16)
 
+    ring_advance(1, (3,))
     with jax.named_scope("key_edge"):
         key_rows(0, QB)
         key_rows(rows - QB, QB)
-    ring_advance(1, (3,))
+    ring_advance(1, (1,))
     with jax.named_scope("key_rest"):
         key_rows(QB, wide)
     for source, target, device in ((rows, 0, after), (WINDOW, WINDOW + rows, before)):
@@ -453,10 +454,9 @@
             sent.at[KH], got.at[KH], device,
         ).start()
     far_advance()
-    ring_advance(1, (1,))
+    ring_advance(1, (2,))
     with jax.named_scope("key_rest"):
         key_rows(QB + wide, wide)
-    ring_advance(1, (2,))
     with jax.named_scope("key_rest"):
         key_rows(QB + 2 * wide, wide)
 

time: 43.9 us -> 44.5 us (1.014)
  Pallas kernels: 41.1 us -> 41.7 us
    pallas_call x1, Pallas kernels: 41.1 us -> 41.7 us  [body(): pl.pallas_call(functools.partial(kernel, rows), name='mixer', out_shape=j...]
where the time goes in v6:
time: 44.5 us; the launch traced here: 44.3 us
  Pallas kernels  41.7 us (94%)
  local copies, waits for them, and re-layouts  1.88 us (4%)
  between operations  0.66 us (1%)
    pallas_call x1, Pallas kernels, body(): pl.pallas_call(functools.partial(kernel, rows), name='mixer', out_shape=j...  41.7 us
    unnamed x1, local copies, waits for them, and re-layouts  1.88 us

profile of v6, /device:TPU:1, one launch (start us, length us, event | category | flops | bytes accessed | tf_op | source)
XLA Modules:
  0.0 44.3 jit_solution(11578568135959722744)
XLA Ops:
  0.7 41.7 %mixer.1 = bf16[128,2048]{1,0:T(8,128)(2,1)} custom-call(bf16[1024,2048]{1,0:T(8,128)(2,1)} %tokens.1, f32[1,2048]{1,0:T(1,128)} %bitcast.9, bf16[64,2048]{1,0:T(8,128)(2,1)} %bitcast.7, bf16[32,128]{1,0:T(8,128)(2,1)} %w_key.1, bf16[32,128]{1,0:T(8,128)(2,1)} %w_value.1, bf16[64,2048]{1,0:T(8,128)(2,1)} %bitcast.8, f32[1,64]{1,0:T(1,128)} %bitcast.11, ...), custom_call_target="tpu_custom_call" | custom-call | tf_op jit(solution)/shard_map/mixer/pallas_call | solution.py:646
  42.4 1.9 %copy.14 = bf16[128,2048]{1,0:T(8,128)(2,1)} copy(bf16[128,2048]{1,0:T(8,128)(2,1)} %mixer.1) | data formatting | bytes 1048576
